TPU v7x, 128 devices: a whole 4x4x4 slice. The times are simulated.
128 devices in a mesh: ep: 32 (over z, y, core), tp: 4 (over x).
Axes of the slice: x: 4, y: 4, z: 4, core: 2. Of those that a mesh axis runs over, the one named last changes fastest.
Arguments:
- mix_in: bfloat16 [16384, 4096], P(('ep', 'tp')), may hold values from -6 to 6
- mix_gain: float32 [4096], replicated, may hold values from 0.1 to 1.9
- proj_b: bfloat16 [4096, 1024], P(None, 'tp'), may hold values from -0.09375 to 0.09375
- proj_c: bfloat16 [4096, 1024], P(None, 'tp'), may hold values from -0.09375 to 0.09375
- proj_h: bfloat16 [4096, 1024], P(None, 'tp'), may hold values from -0.09375 to 0.09375
- conv_taps: bfloat16 [3, 1024], P(None, 'tp'), may hold values from -3.5 to 3.5
- proj_out: bfloat16 [1024, 4096], P('tp'), may hold values from -0.1875 to 0.1875
- moe_in: bfloat16 [16384, 4096], P(('ep', 'tp')), may hold values from -6 to 6
- moe_gain: float32 [4096], replicated, may hold values from 0.1 to 1.9
- routes: int32 [16384, 2], P(('ep', 'tp')), may hold values from 0 to 31, all different within a row; in each aligned block of 128 rows (0 to 127, 128 to 255, ...) at most 14 rows name the same one
- group_logits: float32 [16384, 4], P(('ep', 'tp')), may hold values from -6 to 6
- pair_logits: float32 [16384, 2], P(('ep', 'tp')), may hold values from -6 to 6
- expert_gate: bfloat16 [32, 4096, 2048], P('ep', None, 'tp'), may hold values from -0.09375 to 0.09375
- expert_up: bfloat16 [32, 4096, 2048], P('ep', None, 'tp'), may hold values from -0.09375 to 0.09375
- expert_down: bfloat16 [32, 2048, 4096], P('ep', 'tp'), may hold values from -0.125 to 0.125
Outputs:
- mix_out: bfloat16 [16384, 4096], P(('ep', 'tp'))
- moe_out: bfloat16 [16384, 4096], P(('ep', 'tp'))
Inputs may be any that keep to these rules, and one draw needn't show every extreme that they name: `routes`: each row names 2 different experts. Among the 128 rows of one device no expert is named more than 14 times, and in some device's rows some expert is named exactly 14 times.
All inputs are finite; a program needn't handle non-finite values.
Results may differ from a plain program's by a relative error of at most 0.015.
Values may be sent and summed in bfloat16 or wider, within the bound.
A program may use at most 192 MiB of HBM per device.

v0:
```python
import jax
import jax.numpy as jnp
from jax import lax
from jax.sharding import PartitionSpec as P

GROUPS = 4


def with_halo(cells, sides, width):
    for axis, dim in sides:
        count = lax.axis_size(axis)
        ends = count - 1
        head = lax.slice_in_dim(cells, 0, width, axis=dim)
        tail = lax.slice_in_dim(cells, cells.shape[dim] - width, cells.shape[dim], axis=dim)
        cells = jnp.concatenate(
            [
                lax.ppermute(tail, axis, [(i, (i + 1) % count) for i in range(ends)]),
                cells,
                lax.ppermute(head, axis, [((i + 1) % count, i) for i in range(ends)]),
            ],
            axis=dim,
        )
    return cells


def rms_scaled(values, gain_vec):
    widened = values.astype(jnp.float32)
    scaled = widened * lax.rsqrt(jnp.mean(widened * widened, axis=-1, keepdims=True) + 1e-06)
    return (scaled * gain_vec).astype(jnp.bfloat16)


def rounded_term(product):
    return lax.optimization_barrier(product.astype(jnp.bfloat16)).astype(jnp.float32)


def expert_hidden(arrived, gate_mat, up_mat):
    gate_val = jnp.einsum("sekd,edf->sekf", arrived, gate_mat, preferred_element_type=jnp.float32)
    up_val = jnp.einsum("sekd,edf->sekf", arrived, up_mat, preferred_element_type=jnp.float32)
    return (jax.nn.silu(gate_val) * up_val).astype(jnp.bfloat16)


def body(
    mix_in,
    mix_gain,
    proj_b,
    proj_c,
    proj_h,
    conv_taps,
    proj_out,
    moe_in,
    moe_gain,
    routes,
    group_logits,
    pair_logits,
    expert_gate,
    expert_up,
    expert_down,
):
    mix_norm = rms_scaled(mix_in, mix_gain)
    ch_width = proj_b.shape[1]
    row_piece = lax.all_gather(mix_norm, "tp", axis=0, tiled=True)
    outputs = [
        jnp.dot(row_piece, weight_mat, preferred_element_type=jnp.float32).astype(jnp.bfloat16)
        for weight_mat in (proj_b, proj_c, proj_h)
    ]
    projected = jnp.concatenate(outputs, axis=1)
    gate_b = projected[:, :ch_width]
    padded = with_halo(projected[:, ch_width:], (("ep", 0),), 1)
    conv_in = padded[:, :ch_width].astype(jnp.float32) * padded[:, ch_width:].astype(jnp.float32)
    tap_vals = conv_taps.astype(jnp.float32)
    conv_out = tap_vals[0] * conv_in[:-2] + tap_vals[1] * conv_in[1:-1] + tap_vals[2] * conv_in[2:]
    mixed_rows = (gate_b.astype(jnp.float32) * conv_out).astype(jnp.bfloat16)
    selected = mixed_rows
    mix_out = lax.psum_scatter(
        rounded_term(jnp.dot(selected, proj_out, preferred_element_type=jnp.float32)).astype(
            jnp.bfloat16
        ),
        "tp",
        scatter_dimension=0,
        tiled=True,
    )
    moe_norm = rms_scaled(moe_in, moe_gain)
    local_rows = moe_norm.shape[0]
    model_width = moe_norm.shape[1]
    top_count = routes.shape[1]
    ep_count = lax.axis_size("ep")
    local_experts = expert_gate.shape[0]
    experts_all = local_experts * ep_count
    capacity = max(2, 7 * local_rows // (2 * experts_all))
    flat_routes = routes.reshape(-1)
    route_hits = (flat_routes[:, None] == jnp.arange(experts_all, dtype=jnp.int32)[None, :]).astype(
        jnp.int32
    )
    route_ranks = jnp.sum((jnp.cumsum(route_hits, axis=0) - route_hits) * route_hits, axis=1)
    slot_ids = flat_routes * capacity + route_ranks
    selector = jnp.sum(
        (
            slot_ids.reshape(local_rows, top_count)[:, :, None]
            == jnp.arange(experts_all * capacity, dtype=jnp.int32)[None, None, :]
        ).astype(jnp.bfloat16),
        axis=1,
    )
    outgoing = jnp.einsum(
        "ts,td->sd", selector, moe_norm, preferred_element_type=jnp.float32
    ).astype(jnp.bfloat16)
    outgoing = outgoing.reshape(ep_count, local_experts, capacity, model_width)
    arrived = lax.all_to_all(outgoing, "ep", split_axis=0, concat_axis=0, tiled=True)
    hidden = expert_hidden(
        lax.all_gather(arrived, "tp", axis=0, tiled=True), expert_gate, expert_up
    )
    selected = hidden
    summed = lax.psum_scatter(
        rounded_term(
            jnp.einsum("sekf,efd->sekd", selected, expert_down, preferred_element_type=jnp.float32)
        ).astype(jnp.bfloat16),
        "tp",
        scatter_dimension=0,
        tiled=True,
    )
    returned = lax.all_to_all(summed, "ep", split_axis=0, concat_axis=0, tiled=True)
    expert_out = returned.reshape(experts_all * capacity, model_width).astype(jnp.float32)
    group_prob = jax.nn.softmax(group_logits, axis=-1)
    member = routes // (experts_all // GROUPS)
    picked_prob = jnp.sum(
        group_prob[:, None, :]
        * (member[:, :, None] == jnp.arange(GROUPS, dtype=jnp.int32)[None, None, :]).astype(
            jnp.float32
        ),
        axis=-1,
    )
    weight = picked_prob * jax.nn.softmax(pair_logits, axis=-1)
    picked = jnp.take(expert_out, slot_ids, axis=0).reshape(local_rows, top_count, model_width)
    moe_out = jnp.sum(weight[:, :, None] * picked, axis=1).astype(jnp.bfloat16)
    return (mix_out, moe_out)


def solution(mesh):
    in_specs = (
        P(("ep", "tp"), None),
        P(),
        P(None, "tp"),
        P(None, "tp"),
        P(None, "tp"),
        P(None, "tp"),
        P("tp", None),
        P(("ep", "tp"), None),
        P(),
        P(("ep", "tp"), None),
        P(("ep", "tp"), None),
        P(("ep", "tp"), None),
        P("ep", None, "tp"),
        P("ep", None, "tp"),
        P("ep", "tp", None),
    )
    out_specs = (P(("ep", "tp"), None), P(("ep", "tp"), None))
    return jax.shard_map(body, mesh=mesh, in_specs=in_specs, out_specs=out_specs, check_vma=False)
```

profile of v0, /device:TPU:1, one launch (start us, length us, event | category | flops | bytes accessed | tf_op | source)
XLA Modules:
  0.0 507.6 jit_solution(10682525472767678942)
XLA Ops:
  7.2 0.0 all-gather.5.cloned.1.call-start
  7.2 0.9 copy.78
  8.2 0.1 eq.55
  8.3 0.1 reshape.123
  8.4 0.6 reduce-window.6
  9.0 0.2 slice_reduce_fusion
  9.3 0.1 fusion.48
  9.4 0.1 reduce_sum.84
  9.5 0.1 copy.81
  9.6 0.7 compare_and_fusion
  10.3 0.1 fusion.45
  10.4 1.5 fusion.14
  11.9 4.3 convolution_convert_fusion.1
  16.1 5.0 reshape.125
  21.1 60.3 %all_to_all.10 = bf16[32,1,14,4096]{3,2,1,0:T(8,128)(2,1)S(1)} all-to-all(bf16[32,1,14,4096]{3,2,1,0:T(8,128)(2,1)} %bitcast.104), channel_id=1, replica_groups=mesh['ep'=32,'tp'=4] {'ep'}, dimensions={0} | all-to-all | bytes 7340032 | tf_op jit(solution)/shard_map/all_to_all | solution.py:107
  81.5 3.8 copy.84
  85.3 0.0 all-gather.5.cloned.1.call-update
  85.3 0.0 all-gather.3.cloned.1.call-start
  85.3 1.1 copy-done.1
  86.5 0.3 fusion.11
  86.8 1.3 fusion.13
  88.1 0.2 reduce-scatter.5.cloned.1.call-start
  88.4 130.7 %all-gather.5.cloned.1.call-done = bf16[128,1,14,4096]{3,0,2,1:T(8,128)(2,1)} async-done(((bf16[32,1,14,4096]{3,0,2,1:T(8,128)(2,1)}), bf16[128,1,14,4096]{3,0,2,1:T(8,128)(2,1)}) %all-gather.5.cloned.1.call-update) | async-done | bytes 14680080 | tf_op jit(solution)/shard_map/all_gather | solution.py:109
  219.0 13.4 %fusion.2 = f32[128,14,512]{2,0,1:T(8,128)} fusion(bf16[128,1,14,4096]{3,0,2,1:T(8,128)(2,1)} %all-gather.5.cloned.1.call-done, bf16[1,4096,512]{2,1,0:T(8,128)(2,1)} %param.27), kind=kOutput, calls=%fused_computation.3 | convolution fusion | flops 7516192768 | bytes 22544384 | tf_op jit(solution)/shard_map/sekd,edf->sekf/dot_general | solution.py:37
  232.4 25.2 %convert_bitcast_fusion = bf16[128,1,14,4096]{3,0,2,1:T(8,128)(2,1)} fusion(bf16[1,512,4096]{2,1,0:T(8,128)(2,1)} %param.29, f32[128,14,512]{2,0,1:T(8,128)} %fusion.2, bf16[1,4096,512]{2,1,0:T(8,128)(2,1)} %param.28, bf16[128,1,14,4096]{3,0,2,1:T(8,128)(2,1)} %all-gather.5.cloned.1.call-done), kind=kOutput, calls=%fused_computation.5 | convolution fusion | flops 15045230592 | bytes 41418752 | tf_op jit(solution)/shard_map/sekf,efd->sekd/dot_general | solution.py:114
  257.6 0.0 reduce-scatter.3.cloned.1.call-start
  257.7 12.8 %all-gather.3.cloned.1.call-done = bf16[512,4096]{1,0:T(8,128)(2,1)} async-done(((bf16[128,4096]{1,0:T(8,128)(2,1)}), bf16[512,4096]{1,0:T(8,128)(2,1)}) %all-gather.3.cloned.1.call-update) | async-done | bytes 4194320 | tf_op jit(solution)/shard_map/all_gather | solution.py:61
  270.4 4.2 convolution_convert_fusion.2
  274.7 0.5 copy-done.8
  275.2 1.2 convolution_convert_fusion.3
  276.4 3.8 collective-permute-start
  280.3 2.1 collective-permute-start.1
  282.5 3.1 collective-permute-done.1
  285.6 0.1 pad_maximum_fusion
  285.7 0.1 convert_multiply_fusion.4
  285.8 9.3 %convolution_convert_fusion = bf16[512,4096]{1,0:T(8,128)(2,1)} fusion(bf16[256,4096]{1,0:T(8,128)(2,1)S(1)} %copy-done, bf16[512,4096]{1,0:T(8,128)(2,1)} %all-gather.3.cloned.1.call-done, bf16[4096,256]{1,0:T(8,128)(2,1)} %param.17, f32[514,256]{1,0:T(8,128)S(1)} %convert_multiply_fusion.4, f32[256]{0:T(256)S(1)} %bitcast.109, f32[256]{0:T(256)S(1)} %bitcast.108, ...), kind=kOutput, calls=%fused_computation.6 | convolution fusion | flops 2150760448 | bytes 14158848 | tf_op jit(solution)/shard_map/dot_general | solution.py:75
  295.1 109.7 %reduce-scatter.5.cloned.1.call-done = bf16[32,1,14,4096]{3,0,2,1:T(8,128)(2,1)} async-done(((bf16[128,1,14,4096]{3,0,2,1:T(8,128)(2,1)}), bf16[32,1,14,4096]{3,0,2,1:T(8,128)(2,1)}) %reduce-scatter.5.cloned.1.call-update) | async-done | bytes 3670032 | tf_op jit(solution)/shard_map/reduce_scatter | solution.py:112
  404.9 6.0 %copy.85 = bf16[32,1,14,4096]{3,2,1,0:T(8,128)(2,1)} copy(bf16[32,1,14,4096]{3,0,2,1:T(8,128)(2,1)} %reduce-scatter.5.cloned.1.call-done) | data formatting | bytes 7340032 | tf_op jit(solution)/shard_map/reduce_scatter | solution.py:112
  410.9 7.9 %all-to-all-start.1 = ((bf16[32,1,14,4096]{3,2,1,0:T(8,128)(2,1)}), bf16[32,1,14,4096]{3,2,1,0:T(8,128)(2,1)}, u32[]{:S(2)}, u32[]{:S(2)}) async-start(bf16[32,1,14,4096]{3,2,1,0:T(8,128)(2,1)} %copy.85), calls=%async_computation.3 | async-start | bytes 8388608 | tf_op jit(solution)/shard_map/all_to_all | solution.py:120
  418.8 0.1 copy.86
  418.9 0.1 mul.154
  419.1 0.1 copy.82
  419.4 0.1 copy.77
  419.5 50.0 %all-to-all-done.1 = bf16[32,1,14,4096]{3,2,1,0:T(8,128)(2,1)} async-done(((bf16[32,1,14,4096]{3,2,1,0:T(8,128)(2,1)}), bf16[32,1,14,4096]{3,2,1,0:T(8,128)(2,1)}, u32[]{:S(2)}, u32[]{:S(2)}) %all-to-all-start.1) | async-done | bytes 3670048 | tf_op jit(solution)/shard_map/all_to_all | solution.py:120
  469.5 5.9 %reshape.131 = f32[448,4096]{1,0:T(8,128)} reshape(bf16[32,1,14,4096]{3,2,1,0:T(8,128)(2,1)} %all-to-all-done.1) | data formatting | bytes 11010048 | tf_op jit(solution)/shard_map/convert_element_type | solution.py:121
  475.4 8.9 %gather_fusion = f32[256,4096]{1,0:T(8,128)} fusion(f32[448,4096]{1,0:T(8,128)} %reshape.131, s32[1024]{0:T(1024)S(1)} %pad_clamp_fusion), kind=kCustom, calls=%fused_computation | custom fusion | bytes 8389632 | tf_op jit(solution)/shard_map/jit(_take)/gather | solution.py:132
  484.2 5.8 %gather.7 = f32[128,2,4096]{2,1,0:T(2,128)} reshape(f32[256,4096]{1,0:T(8,128)} %gather_fusion) | data formatting | bytes 8388608 | tf_op jit(solution)/shard_map/jit(_take)/gather | solution.py:132
  490.1 11.0 %multiply_reduce_fusion = bf16[128,4096]{1,0:T(8,128)(2,1)} fusion(f32[128,2,4096]{2,1,0:T(2,128)} %gather.7, pred[128,2]{1,0:T(8,128)(4,1)S(1)} %copy.82, f32[128,2]{1,0:T(8,128)S(1)} %copy.77), kind=kLoop, calls=%fused_computation.11 | loop fusion | flops 2621440 | bytes 5244160 | tf_op jit(solution)/shard_map/reduce_sum | solution.py:133
  (38 shorter events, 0.3 us)
Async XLA Ops:
  7.2 278.6 %copy-start = (bf16[256,4096]{1,0:T(8,128)(2,1)S(1)}, bf16[256,4096]{1,0:T(8,128)(2,1)}, u32[]{:S(2)}) copy-start(bf16[256,4096]{1,0:T(8,128)(2,1)} %param.21) | copy-start | bytes 6291460
  7.2 211.8 %all-gather.5.cloned.1.call-start = ((), (), s32[]{:S(2)}) async-start(), calls=%async_computation.6 | async-start | bytes 18350080 | tf_op jit(solution)/shard_map/all_gather | solution.py:109
  85.3 1.2 copy-start.1
  85.3 1.5 copy-start.3
  85.3 185.1 %all-gather.3.cloned.1.call-start = ((), (), s32[]{:S(2)}) async-start(), calls=%async_computation.4 | async-start | bytes 5242880 | tf_op jit(solution)/shard_map/all_gather | solution.py:61
  88.1 316.7 %reduce-scatter.5.cloned.1.call-start = ((), (), s32[]{:S(2)}) async-start(), calls=%async_computation.7 | async-start | bytes 18350080 | tf_op jit(solution)/shard_map/reduce_scatter | solution.py:112
  257.6 243.4 %reduce-scatter.3.cloned.1.call-start = ((), (), s32[]{:S(2)}) async-start(), calls=%async_computation.5 | async-start | bytes 5242880 | tf_op jit(solution)/shard_map/reduce_scatter | solution.py:74
  270.4 4.3 copy-start.7
  270.4 4.7 copy-start.8
  275.2 7.3 %copy-start.6 = (bf16[3,256]{1,0:T(4,128)(2,1)S(1)}, bf16[3,256]{1,0:T(4,128)(2,1)}, u32[]{:S(2)}) copy-start(bf16[3,256]{1,0:T(4,128)(2,1)} %param.20) | copy-start | bytes 4612
  276.4 6.0 %collective-permute-start = (bf16[1,512]{1,0:T(2,128)(2,1)S(1)}, bf16[1,512]{1,0:T(2,128)(2,1)S(1)}, u32[]{:S(2)}, u32[]{:S(2)}) collective-permute-start(bf16[1,512]{1,0:T(2,128)(2,1)S(1)} %get-tuple-element.4), channel_id=1, source_target_pairs={{0,4},{4,8},{8,12},{12,16},{16,20},{20,24},{24,28},{28,32},{32,36}... | collective-permute-start | bytes 3080 | tf_op jit(solution)/shard_map/ppermute | solution.py:17
  280.3 5.3 %collective-permute-start.1 = (bf16[1,512]{1,0:T(2,128)(2,1)S(1)}, bf16[1,512]{1,0:T(2,128)(2,1)S(1)}, u32[]{:S(2)}, u32[]{:S(2)}) collective-permute-start(bf16[1,512]{1,0:T(2,128)(2,1)S(1)} %get-tuple-element.5), channel_id=1, source_target_pairs={{4,0},{8,4},{12,8},{16,12},{20,16},{24,20},{28,24},{32,28},{36,32}... | collective-permute-start | bytes 3080 | tf_op jit(solution)/shard_map/ppermute | solution.py:19
  410.8 8.0 %copy-start.4 = (s32[128,2]{0,1:T(2,128)S(1)}, s32[128,2]{0,1:T(2,128)}, u32[]{:S(2)}) copy-start(s32[128,2]{0,1:T(2,128)} %param.24) | copy-start | bytes 3076
  410.9 8.4 %copy-start.2 = (f32[128,4]{0,1:T(4,128)S(1)}, f32[128,4]{0,1:T(4,128)}, u32[]{:S(2)}) copy-start(f32[128,4]{0,1:T(4,128)} %param.25) | copy-start | bytes 6148
  410.9 8.4 %copy-start.5 = (f32[128,2]{0,1:T(2,128)S(1)}, f32[128,2]{0,1:T(2,128)}, u32[]{:S(2)}) copy-start(f32[128,2]{0,1:T(2,128)} %param.26) | copy-start | bytes 3076
  410.9 58.6 %all-to-all-start.1 = ((bf16[32,1,14,4096]{3,2,1,0:T(8,128)(2,1)}), bf16[32,1,14,4096]{3,2,1,0:T(8,128)(2,1)}, u32[]{:S(2)}, u32[]{:S(2)}) async-start(bf16[32,1,14,4096]{3,2,1,0:T(8,128)(2,1)} %copy.85), calls=%async_computation.3 | async-start | bytes 8388608 | tf_op jit(solution)/shard_map/all_to_all | solution.py:120
Sparse Core Ops, SparseCore 0:
  85.4 133.5 all-gather.4
  221.3 49.1 all-gather.2
  272.9 131.9 reduce-scatter.4
  407.7 46.5 reduce-scatter.2
where the time goes:
time: 511 us; the launch traced here: 508 us
  waiting for transfers between devices  306 us (60%)
  blocking collectives  60.3 us (12%)
  matrix products  57.6 us (11%)
  local copies, waits for them, and re-layouts  39.1 us (8%)
  other arithmetic  15.9 us (3%)
  starting transfers between devices  14.3 us (3%)
  between operations  14 us (3%)
    all_gather x1, waiting for transfers between devices, body(): lax.all_gather(arrived, 'tp', axis=0, tiled=True)  131 us
    reduce_scatter x1, waiting for transfers between devices, body(): lax.psum_scatter(rounded_term(jnp.einsum('sekf,efd->sekd', selected, expe...  110 us
    all_to_all x1, blocking collectives, body(): lax.all_to_all(outgoing, 'ep', split_axis=0, concat_axis=0, tiled=True)  60.3 us
    all_to_all x1, waiting for transfers between devices, body(): lax.all_to_all(summed, 'ep', split_axis=0, concat_axis=0, tiled=True)  50 us
    dot_general x1, matrix products, body(): jnp.einsum('sekf,efd->sekd', selected, expert_down, preferred_element_typ...  25.2 us
    gather x2, local copies, waits for them, and re-layouts, body(): jnp.take(expert_out, slot_ids, axis=0)  14.7 us
    dot_general x1, matrix products, expert_hidden(): jnp.einsum('sekd,edf->sekf', arrived, gate_mat, preferred_element_type=jn...  13.4 us
    all_gather x1, waiting for transfers between devices, body(): row_piece = lax.all_gather(mix_norm, 'tp', axis=0, tiled=True)  12.8 us
  transfers between devices with their start and end apart: 7, of which 5 were waited for; matrix products, arithmetic and copies ran while one was open for 18% of the time, Pallas kernels for 0%

commit v1 on v0

v1 whole, which is shorter than its diff:
```python
import jax
import jax.numpy as jnp
from jax import lax
from jax.experimental import pallas as pl
from jax.experimental.pallas import tpu as pltpu
from jax.sharding import PartitionSpec as P

GROUPS = 4
BF = jnp.bfloat16
F32 = jnp.float32
MESH = pl.DeviceIdType.MESH
SLOT = 16
NA = 18
NB = 14
NC = 4
PER = 3


def with_halo(cells, sides, width):
    for axis, dim in sides:
        count = lax.axis_size(axis)
        ends = count - 1
        head = lax.slice_in_dim(cells, 0, width, axis=dim)
        tail = lax.slice_in_dim(cells, cells.shape[dim] - width, cells.shape[dim], axis=dim)
        cells = jnp.concatenate(
            [
                lax.ppermute(tail, axis, [(i, (i + 1) % count) for i in range(ends)]),
                cells,
                lax.ppermute(head, axis, [((i + 1) % count, i) for i in range(ends)]),
            ],
            axis=dim,
        )
    return cells


def rms_scaled(values, gain_vec):
    widened = values.astype(F32)
    scaled = widened * lax.rsqrt(jnp.mean(widened * widened, axis=-1, keepdims=True) + 1e-06)
    return (scaled * gain_vec).astype(BF)


def tri(k):
    return (k * (k + 1)) // 2


def at_a(me, o, sign):
    z, y, c = me // 8, (me // 2) % 4, me % 2
    dz, dy, dc = tri(o // 6), tri((o // 2) % 3), o % 2
    return (((z + sign * dz + 4) % 4) * 4 + (y + sign * dy + 4) % 4) * 2 + (c + dc) % 2


def at_b(me, o, sign):
    z, y, c = me // 8, (me // 2) % 4, me % 2
    k = o // 2
    hi = k // 4
    dz = (1 - hi) * 2 + hi * tri(k - 4 * hi)
    dy = (1 - hi) * k + hi * 2
    return (((z + sign * dz + 4) % 4) * 4 + (y + sign * dy + 4) % 4) * 2 + (c + o % 2) % 2


def greet(me, x):
    barrier = pltpu.get_barrier_semaphore()

    def tell_a(o, _):
        pl.semaphore_signal(barrier, inc=1, device_id=(at_a(me, o, 1), x), device_id_type=MESH)
        return 0

    def tell_b(o, _):
        pl.semaphore_signal(barrier, inc=1, device_id=(at_b(me, o, 1), x), device_id_type=MESH)
        return 0

    lax.fori_loop(1, NA, tell_a, 0)
    lax.fori_loop(0, NB, tell_b, 0)
    pl.semaphore_signal(barrier, inc=1, device_id=(me, (x + 1) % 4), device_id_type=MESH)
    pl.semaphore_signal(barrier, inc=1, device_id=(me, (x + 3) % 4), device_id_type=MESH)
    pl.semaphore_wait(barrier, NA - 1 + NB + 2)


def remote(src, dst, send, recv, ep, tp):
    return pltpu.make_async_remote_copy(
        src_ref=src, dst_ref=dst, send_sem=send, recv_sem=recv, device_id=(ep, tp), device_id_type=MESH
    )


def slot_rows(base, rows, meta, hit0, hit1):
    want = lax.broadcasted_iota(jnp.int32, (rows, meta.shape[1]), 0) + base
    want = want.astype(F32)
    return jnp.where(meta[0:1] == want, hit0, 0.0) + jnp.where(meta[1:2] == want, hit1, 0.0)


def dispatch_kernel(
    norm, meta, gate_hbm, up_hbm,
    hid_a, hid_b, metas_out,
    tok, metas, oh_a, oh_b, out_a, out_b, recv_a, recv_b, gate_w, up_w, acc_g, acc_u, bcc_g, bcc_u,
    tok_s, tok_r, tokf_s, tokf_r, b_s, b_r, bx_s, bx_r, bf_s, bf_r, a_s, a_r, meta_s, meta_r, w_sem,
):
    me = lax.axis_index("ep")
    x = lax.axis_index("tp")
    right, left = (x + 1) % 4, (x + 3) % 4
    cw = tok.shape[3]
    rows = tok.shape[2]
    half = rows // 2
    hb = NB // 2
    gate_in = pltpu.make_async_copy(gate_hbm, gate_w, w_sem.at[0])
    up_in = pltpu.make_async_copy(up_hbm, up_w, w_sem.at[1])
    gate_in.start()
    up_in.start()
    greet(me, x)

    def cols(c):
        return pl.ds(pl.multiple_of(c * cw, cw), cw)

    meta_right = remote(meta, metas.at[1], meta_s.at[0], meta_r.at[0], me, right)
    meta_left = remote(meta, metas.at[2], meta_s.at[1], meta_r.at[1], me, left)
    meta_on = remote(metas.at[1], metas.at[3], meta_s.at[2], meta_r.at[2], me, right)
    meta_right.start()
    meta_left.start()

    def tok_right(c):
        return remote(norm.at[:, cols(c)], tok.at[c, 0], tok_s.at[c, 0], tok_r.at[c, 0], me, right)

    def tok_left(c):
        return remote(norm.at[:, cols(c)], tok.at[c, 1], tok_s.at[c, 1], tok_r.at[c, 1], me, left)

    def tok_on_right(c):
        return remote(tok.at[c, 0, pl.ds(0, half)], tok.at[c, 2, pl.ds(0, half)], tokf_s.at[c, 0], tokf_r.at[c, 0], me, right)

    def tok_on_left(c):
        return remote(tok.at[c, 1, pl.ds(half, half)], tok.at[c, 2, pl.ds(half, half)], tokf_s.at[c, 1], tokf_r.at[c, 1], me, left)

    def b_right(c):
        return remote(recv_b.at[c, 0], recv_b.at[c, 1], bx_s.at[c, 0], bx_r.at[c, 0], me, right)

    def b_left(c):
        return remote(recv_b.at[c, 0], recv_b.at[c, 2], bx_s.at[c, 1], bx_r.at[c, 1], me, left)

    def b_on_right(c):
        return remote(recv_b.at[c, 1, pl.ds(0, hb)], recv_b.at[c, 3, pl.ds(0, hb)], bf_s.at[c, 0], bf_r.at[c, 0], me, right)

    def b_on_left(c):
        return remote(recv_b.at[c, 2, pl.ds(hb, hb)], recv_b.at[c, 3, pl.ds(hb, hb)], bf_s.at[c, 1], bf_r.at[c, 1], me, left)

    def a_all(c):
        span = pl.ds(1, NA - 1)
        return remote(out_a.at[c, span], recv_a.at[c, span], a_s.at[c], a_r.at[c], me, right)

    def b_all(c):
        return remote(out_b.at[c], recv_b.at[c, 0], b_s.at[c], b_r.at[c], me, right)

    def first(c, _):
        tok_right(c).start()
        tok_left(c).start()
        return 0

    lax.fori_loop(0, NC, first, 0)

    own = meta[...]

    def hits_b(o, _):
        oh_b[o] = slot_rows(at_b(me, o, 1) * SLOT, SLOT, own, 1.0, 1.0).astype(BF)
        return 0

    lax.fori_loop(0, NB, hits_b, 0)

    def second(c, _):
        picked = jnp.dot(oh_b[...].reshape(NB * SLOT, rows), norm[:, cols(c)], preferred_element_type=F32)
        out_b[c] = picked.astype(BF).reshape(NB, SLOT, cw)

        def send(o, _):
            remote(out_b.at[c, o], recv_b.at[c, 0, o], b_s.at[c], b_r.at[c], at_b(me, o, 1), x).start()
            return 0

        lax.fori_loop(0, NB, send, 0)
        return 0

    lax.fori_loop(0, NC, second, 0)

    meta_right.wait()
    meta_on.start()
    meta_left.wait()
    meta_on.wait()
    metas[0] = own
    metas_out[...] = metas[...]

    def hits_a(o, _):
        base = at_a(me, o, 1) * SLOT
        for r in range(4):
            oh_a[r, o] = slot_rows(base, SLOT, metas_out[r], 1.0, 1.0).astype(BF)
        return 0

    lax.fori_loop(0, NA, hits_a, 0)

    def third(c, _):
        def pick(r, values):
            picked = jnp.dot(oh_a[r].reshape(NA * SLOT, rows), values, preferred_element_type=F32).astype(BF)
            picked = picked.reshape(NA, SLOT, cw)
            recv_a[c, 0, r] = picked[0]
            out_a[c, 1:, r] = picked[1:]

        pick(0, norm[:, cols(c)])
        tok_right(c).wait_recv()
        tok_on_right(c).start()
        tok_left(c).wait_recv()
        tok_on_left(c).start()
        pick(1, tok[c, 0])
        pick(2, tok[c, 1])
        tok_on_right(c).wait_recv()
        tok_on_left(c).wait_recv()
        pick(3, tok[c, 2])

        def send(o, _):
            remote(out_a.at[c, o], recv_a.at[c, o], a_s.at[c], a_r.at[c], at_a(me, o, 1), x).start()
            return 0

        lax.fori_loop(1, NA, send, 0)
        b_all(c).wait_recv()
        b_right(c).start()
        b_left(c).start()
        return 0

    lax.fori_loop(0, NC, third, 0)

    def fourth(c, _):
        b_right(c).wait_recv()
        b_on_right(c).start()
        b_left(c).wait_recv()
        b_on_left(c).start()
        return 0

    lax.fori_loop(0, NC, fourth, 0)
    gate_in.wait()
    up_in.wait()

    def finish(gate_val, up_val):
        return (gate_val / (1.0 + jnp.exp(-gate_val)) * up_val).astype(BF)

    for c in range(NC):
        a_all(c).wait_recv()

        def step_a(t, _, c=c):
            values = recv_a[c, pl.ds(t * PER, PER)].reshape(PER * 4 * SLOT, cw)
            g = jnp.dot(values, gate_w[c * cw:(c + 1) * cw], preferred_element_type=F32)
            u = jnp.dot(values, up_w[c * cw:(c + 1) * cw], preferred_element_type=F32)
            if c > 0:
                g = g + acc_g[t]
                u = u + acc_u[t]
            if c < NC - 1:
                acc_g[t] = g
                acc_u[t] = u
            else:
                hid_a[pl.ds(t * PER, PER)] = finish(g, u).reshape(PER, 4, SLOT, g.shape[1])
            return 0

        lax.fori_loop(0, NA // PER, step_a, 0)

    for c in range(NC):
        b_on_right(c).wait_recv()
        b_on_left(c).wait_recv()

        def step_b(r, _, c=c):
            values = recv_b[c, r].reshape(NB * SLOT, cw)
            g = jnp.dot(values, gate_w[c * cw:(c + 1) * cw], preferred_element_type=F32)
            u = jnp.dot(values, up_w[c * cw:(c + 1) * cw], preferred_element_type=F32)
            if c > 0:
                g = g + bcc_g[r]
                u = u + bcc_u[r]
            if c < NC - 1:
                bcc_g[r] = g
                bcc_u[r] = u
            else:
                hid_b[r] = finish(g, u).reshape(NB, SLOT, g.shape[1])
            return 0

        lax.fori_loop(0, 4, step_b, 0)

    def drain(c, _):
        tok_right(c).wait_send()
        tok_left(c).wait_send()
        tok_on_right(c).wait_send()
        tok_on_left(c).wait_send()
        b_all(c).wait_send()
        b_right(c).wait_send()
        b_left(c).wait_send()
        b_on_right(c).wait_send()
        b_on_left(c).wait_send()
        a_all(c).wait_send()
        return 0

    lax.fori_loop(0, NC, drain, 0)


def combine_kernel(
    hid_a, hid_b, metas, down_hbm,
    out,
    down_w, p_a, p_b, bh_in, bf_in, sum_b, ret_a, ret_b, w_a, w_b, p_t, th_in, tf_in, acc,
    bh_s, bh_r, bf_s, bf_r, b_s, b_r, a_s, a_r, th_s, th_r, tf_s, tf_r, w_sem,
):
    me = lax.axis_index("ep")
    x = lax.axis_index("tp")
    right, left = (x + 1) % 4, (x + 3) % 4
    cw = p_a.shape[4]
    rows = p_t.shape[2]
    half = rows // 2
    hb = NB // 2
    down_in = pltpu.make_async_copy(down_hbm, down_w, w_sem)
    down_in.start()
    greet(me, x)

    def cols(c):
        return pl.ds(pl.multiple_of(c * cw, cw), cw)

    def bh_right(c):
        return remote(p_b.at[c, 3, pl.ds(0, hb)], bh_in.at[c, 0], bh_s.at[c, 0], bh_r.at[c, 0], me, right)

    def bh_left(c):
        return remote(p_b.at[c, 3, pl.ds(hb, hb)], bh_in.at[c, 1], bh_s.at[c, 1], bh_r.at[c, 1], me, left)

    def bf_right(c):
        return remote(p_b.at[c, 2], bf_in.at[c, 0], bf_s.at[c, 0], bf_r.at[c, 0], me, right)

    def bf_left(c):
        return remote(p_b.at[c, 1], bf_in.at[c, 1], bf_s.at[c, 1], bf_r.at[c, 1], me, left)

    def th_right(c):
        return remote(p_t.at[c, 3, pl.ds(0, half)], th_in.at[c, 0], th_s.at[c, 0], th_r.at[c, 0], me, right)

    def th_left(c):
        return remote(p_t.at[c, 3, pl.ds(half, half)], th_in.at[c, 1], th_s.at[c, 1], th_r.at[c, 1], me, left)

    def tf_right(c):
        return remote(p_t.at[c, 2], tf_in.at[c, 0], tf_s.at[c, 0], tf_r.at[c, 0], me, right)

    def tf_left(c):
        return remote(p_t.at[c, 1], tf_in.at[c, 1], tf_s.at[c, 1], tf_r.at[c, 1], me, left)

    def a_all(c):
        span = pl.ds(1, NA - 1)
        return remote(p_a.at[c, span], ret_a.at[c, span], a_s.at[c], a_r.at[c], me, right)

    def b_all(c):
        return remote(sum_b.at[c], ret_b.at[c], b_s.at[c], b_r.at[c], me, right)

    down_in.wait()

    def first(c, _):
        def one(r, _):
            part = jnp.dot(hid_b[r].reshape(NB * SLOT, hid_b.shape[3]), down_w[:, cols(c)], preferred_element_type=F32)
            p_b[c, r] = part.astype(BF).reshape(NB, SLOT, cw)
            return 0

        lax.fori_loop(0, 4, one, 0)
        bh_right(c).start()
        bh_left(c).start()
        return 0

    lax.fori_loop(0, NC, first, 0)

    def second(c, _):
        def one(t, _):
            span = pl.ds(t * PER, PER)
            values = hid_a[span].reshape(PER * 4 * SLOT, hid_a.shape[3])
            part = jnp.dot(values, down_w[:, cols(c)], preferred_element_type=F32)
            p_a[c, span] = part.astype(BF).reshape(PER, 4, SLOT, cw)
            return 0

        lax.fori_loop(0, NA // PER, one, 0)

        def send(o, _):
            remote(p_a.at[c, o], ret_a.at[c, o], a_s.at[c], a_r.at[c], at_a(me, o, -1), x).start()
            return 0

        lax.fori_loop(1, NA, send, 0)
        ret_a[c, 0] = p_a[c, 0]
        bh_right(c).wait_recv()
        p_b[c, 2, :hb] = (p_b[c, 2, :hb].astype(F32) + bh_in[c, 0].astype(F32)).astype(BF)
        bf_right(c).start()
        bh_left(c).wait_recv()
        p_b[c, 1, hb:] = (p_b[c, 1, hb:].astype(F32) + bh_in[c, 1].astype(F32)).astype(BF)
        bf_left(c).start()
        return 0

    lax.fori_loop(0, NC, second, 0)

    def hits_a(o, _):
        base = at_a(me, o, 1) * SLOT
        for r in range(4):
            meta = metas[r]
            w_a[r, o] = slot_rows(base, SLOT, meta, meta[2:3], meta[3:4]).astype(BF)
        return 0

    lax.fori_loop(0, NA, hits_a, 0)

    def hits_b(o, _):
        meta = metas[0]
        w_b[o] = slot_rows(at_b(me, o, 1) * SLOT, SLOT, meta, meta[2:3], meta[3:4]).astype(BF)
        return 0

    lax.fori_loop(0, NB, hits_b, 0)

    def third(c, _):
        bf_right(c).wait_recv()
        bf_left(c).wait_recv()
        total = p_b[c, 0].astype(F32) + bf_in[c, 0].astype(F32) + bf_in[c, 1].astype(F32)
        sum_b[c] = total.astype(BF)

        def send(o, _):
            remote(sum_b.at[c, o], ret_b.at[c, o], b_s.at[c], b_r.at[c], at_b(me, o, -1), x).start()
            return 0

        lax.fori_loop(0, NB, send, 0)
        return 0

    lax.fori_loop(0, NC, third, 0)
    over_rows = (((0,), (0,)), ((), ()))

    def fourth(c, _):
        a_all(c).wait_recv()

        def weighed(r):
            values = ret_a[c, :, r].reshape(NA * SLOT, cw)
            return lax.dot_general(w_a[r].reshape(NA * SLOT, rows), values, over_rows, preferred_element_type=F32)

        p_t[c, 3] = weighed(3).astype(BF)
        th_right(c).start()
        th_left(c).start()
        p_t[c, 1] = weighed(1).astype(BF)
        p_t[c, 2] = weighed(2).astype(BF)
        acc[c] = weighed(0)
        th_right(c).wait_recv()
        p_t[c, 2, :half] = (p_t[c, 2, :half].astype(F32) + th_in[c, 0].astype(F32)).astype(BF)
        tf_right(c).start()
        th_left(c).wait_recv()
        p_t[c, 1, half:] = (p_t[c, 1, half:].astype(F32) + th_in[c, 1].astype(F32)).astype(BF)
        tf_left(c).start()
        return 0

    lax.fori_loop(0, NC, fourth, 0)

    def fifth(c, _):
        b_all(c).wait_recv()
        values = ret_b[c].reshape(NB * SLOT, cw)
        total = acc[c] + lax.dot_general(w_b[...].reshape(NB * SLOT, rows), values, over_rows, preferred_element_type=F32)
        tf_right(c).wait_recv()
        tf_left(c).wait_recv()
        total = total + tf_in[c, 0].astype(F32) + tf_in[c, 1].astype(F32)
        out[:, cols(c)] = total.astype(BF)
        return 0

    lax.fori_loop(0, NC, fifth, 0)

    def drain(c, _):
        bh_right(c).wait_send()
        bh_left(c).wait_send()
        bf_right(c).wait_send()
        bf_left(c).wait_send()
        th_right(c).wait_send()
        th_left(c).wait_send()
        tf_right(c).wait_send()
        tf_left(c).wait_send()
        a_all(c).wait_send()
        b_all(c).wait_send()
        return 0

    lax.fori_loop(0, NC, drain, 0)


VM = pltpu.VMEM
DMA = pltpu.SemaphoreType.DMA


def dispatch(norm, meta, gate_mat, up_mat):
    rows, width = norm.shape
    hidden = gate_mat.shape[1]
    cw = width // NC
    vmem = pl.BlockSpec(memory_space=VM)
    anywhere = pl.BlockSpec(memory_space=pl.ANY)
    return pl.pallas_call(
        dispatch_kernel,
        name="dispatch",
        out_shape=(
            jax.ShapeDtypeStruct((NA, 4, SLOT, hidden), BF),
            jax.ShapeDtypeStruct((4, NB, SLOT, hidden), BF),
            jax.ShapeDtypeStruct((4,) + meta.shape, F32),
        ),
        in_specs=[vmem, vmem, anywhere, anywhere],
        out_specs=(vmem, vmem, vmem),
        scratch_shapes=[
            VM((NC, 3, rows, cw), BF),
            VM((4,) + meta.shape, F32),
            VM((4, NA, SLOT, rows), BF),
            VM((NB, SLOT, rows), BF),
            VM((NC, NA, 4, SLOT, cw), BF),
            VM((NC, NB, SLOT, cw), BF),
            VM((NC, NA, 4, SLOT, cw), BF),
            VM((NC, 4, NB, SLOT, cw), BF),
            VM((width, hidden), BF),
            VM((width, hidden), BF),
            VM((NA // PER, PER * 4 * SLOT, hidden), F32),
            VM((NA // PER, PER * 4 * SLOT, hidden), F32),
            VM((4, NB * SLOT, hidden), F32),
            VM((4, NB * SLOT, hidden), F32),
            DMA((NC, 2)), DMA((NC, 2)), DMA((NC, 2)), DMA((NC, 2)),
            DMA((NC,)), DMA((NC,)),
            DMA((NC, 2)), DMA((NC, 2)), DMA((NC, 2)), DMA((NC, 2)),
            DMA((NC,)), DMA((NC,)),
            DMA((3,)), DMA((3,)), DMA((2,)),
        ],
        compiler_params=pltpu.CompilerParams(
            collective_id=0, has_side_effects=True, vmem_limit_bytes=64 * 1024 * 1024 - 65536
        ),
        cost_estimate=pl.CostEstimate(flops=100_000_000_000, bytes_accessed=12_000_000, transcendentals=0),
    )(norm, meta, gate_mat, up_mat)


def combine(hid_a, hid_b, metas, down_mat):
    rows = metas.shape[2]
    hidden, width = down_mat.shape
    cw = width // NC
    hb = NB // 2
    vmem = pl.BlockSpec(memory_space=VM)
    anywhere = pl.BlockSpec(memory_space=pl.ANY)
    return pl.pallas_call(
        combine_kernel,
        name="combine",
        out_shape=jax.ShapeDtypeStruct((rows, width), BF),
        in_specs=[vmem, vmem, vmem, anywhere],
        out_specs=vmem,
        scratch_shapes=[
            VM((hidden, width), BF),
            VM((NC, NA, 4, SLOT, cw), BF),
            VM((NC, 4, NB, SLOT, cw), BF),
            VM((NC, 2, hb, SLOT, cw), BF),
            VM((NC, 2, NB, SLOT, cw), BF),
            VM((NC, NB, SLOT, cw), BF),
            VM((NC, NA, 4, SLOT, cw), BF),
            VM((NC, NB, SLOT, cw), BF),
            VM((4, NA, SLOT, rows), BF),
            VM((NB, SLOT, rows), BF),
            VM((NC, 4, rows, cw), BF),
            VM((NC, 2, rows // 2, cw), BF),
            VM((NC, 2, rows, cw), BF),
            VM((NC, rows, cw), F32),
            DMA((NC, 2)), DMA((NC, 2)), DMA((NC, 2)), DMA((NC, 2)),
            DMA((NC,)), DMA((NC,)), DMA((NC,)), DMA((NC,)),
            DMA((NC, 2)), DMA((NC, 2)), DMA((NC, 2)), DMA((NC, 2)),
            DMA,
        ],
        compiler_params=pltpu.CompilerParams(
            collective_id=1, has_side_effects=True, vmem_limit_bytes=64 * 1024 * 1024 - 65536
        ),
        cost_estimate=pl.CostEstimate(flops=100_000_000_000, bytes_accessed=12_000_000, transcendentals=0),
    )(hid_a, hid_b, metas, down_mat)


def body(
    mix_in, mix_gain, proj_b, proj_c, proj_h, conv_taps, proj_out,
    moe_in, moe_gain, routes, group_logits, pair_logits, expert_gate, expert_up, expert_down,
):
    mix_norm = rms_scaled(mix_in, mix_gain)
    ch_width = proj_b.shape[1]
    row_piece = lax.all_gather(mix_norm, "tp", axis=0, tiled=True)

    moe_norm = rms_scaled(moe_in, moe_gain)
    local_rows, top_count = routes.shape
    experts_all = lax.axis_size("ep")
    flat_routes = routes.reshape(-1)
    route_hits = (flat_routes[:, None] == jnp.arange(experts_all, dtype=jnp.int32)[None, :]).astype(jnp.int32)
    route_ranks = jnp.sum((jnp.cumsum(route_hits, axis=0) - route_hits) * route_hits, axis=1)
    slot_ids = (flat_routes * SLOT + route_ranks).reshape(local_rows, top_count)
    group_prob = jax.nn.softmax(group_logits, axis=-1)
    member = routes // (experts_all // GROUPS)
    picked_prob = jnp.sum(
        group_prob[:, None, :]
        * (member[:, :, None] == jnp.arange(GROUPS, dtype=jnp.int32)[None, None, :]).astype(F32),
        axis=-1,
    )
    weight = picked_prob * jax.nn.softmax(pair_logits, axis=-1)
    meta = jnp.concatenate([slot_ids.astype(F32), weight, jnp.zeros((local_rows, 4), F32)], axis=1).T

    hid_a, hid_b, metas = dispatch(moe_norm, meta, expert_gate[0], expert_up[0])

    outputs = [
        jnp.dot(row_piece, weight_mat, preferred_element_type=F32).astype(BF)
        for weight_mat in (proj_b, proj_c, proj_h)
    ]
    projected = jnp.concatenate(outputs, axis=1)
    gate_b = projected[:, :ch_width]
    padded = with_halo(projected[:, ch_width:], (("ep", 0),), 1)
    conv_in = padded[:, :ch_width].astype(F32) * padded[:, ch_width:].astype(F32)
    tap_vals = conv_taps.astype(F32)
    conv_out = tap_vals[0] * conv_in[:-2] + tap_vals[1] * conv_in[1:-1] + tap_vals[2] * conv_in[2:]
    mixed_rows = (gate_b.astype(F32) * conv_out).astype(BF)
    mix_out = lax.psum_scatter(
        jnp.dot(mixed_rows, proj_out, preferred_element_type=F32).astype(BF),
        "tp",
        scatter_dimension=0,
        tiled=True,
    )
    moe_out = combine(hid_a, hid_b, metas, expert_down[0])
    return (mix_out, moe_out)


def solution(mesh):
    in_specs = (
        P(("ep", "tp"), None), P(), P(None, "tp"), P(None, "tp"), P(None, "tp"), P(None, "tp"), P("tp", None),
        P(("ep", "tp"), None), P(), P(("ep", "tp"), None), P(("ep", "tp"), None), P(("ep", "tp"), None),
        P("ep", None, "tp"), P("ep", None, "tp"), P("ep", "tp", None),
    )
    out_specs = (P(("ep", "tp"), None), P(("ep", "tp"), None))
    return jax.shard_map(body, mesh=mesh, in_specs=in_specs, out_specs=out_specs, check_vma=False)
```

time: 511 us -> 358 us (0.70)
  waiting for transfers between devices: 306 us -> 0.58 us
  Pallas kernels: 0 us -> 305 us
  blocking collectives: 60.3 us -> 0 us
  matrix products: 57.6 us -> 14.8 us
  local copies, waits for them, and re-layouts: 39.1 us -> 3.58 us
  other arithmetic: 15.9 us -> 7.49 us
  starting transfers between devices: 14.3 us -> 8.81 us
    pallas_call x0 -> x2, Pallas kernels: none -> 305 us  [the longest x1 161 us: dispatch(): pl.pallas_call(dispatch_kernel, name='dispatch', out_shape=(jax.ShapeDtyp...]
    all_gather x1 -> x0, waiting for transfers between devices: 131 us -> none  [body(): lax.all_gather(arrived, 'tp', axis=0, tiled=True)]
    reduce_scatter x2 -> x1, waiting for transfers between devices: 110 us -> 0.02 us  [body(): lax.psum_scatter(jnp.dot(mixed_rows, proj_out, preferred_element_type=F32...]
    all_to_all x1 -> x0, blocking collectives: 60.3 us -> none  [body(): lax.all_to_all(outgoing, 'ep', split_axis=0, concat_axis=0, tiled=True)]
    all_to_all x1 -> x0, waiting for transfers between devices: 50 us -> none  [body(): lax.all_to_all(summed, 'ep', split_axis=0, concat_axis=0, tiled=True)]
    dot_general x6 -> x3, matrix products: 57.6 us -> 14.8 us  [the longest x1 9.32 us: body(): jnp.dot(mixed_rows, proj_out, preferred_element_type=F32).astype(BF)]
    gather x2 -> x0, local copies, waits for them, and re-layouts: 14.7 us -> none  [body(): jnp.take(expert_out, slot_ids, axis=0)]
    all_gather x1, waiting for transfers between devices: 12.8 us -> 0.02 us  [body(): row_piece = lax.all_gather(mix_norm, 'tp', axis=0, tiled=True)]
  transfers between devices with their start and end apart: 7 -> 4, of which waited for: 5 -> 1; matrix products, arithmetic and copies ran while one was open for 18% -> 1% of each run, Pallas kernels for 0% -> 86%
where the time goes in v1:
time: 358 us; the launch traced here: 355 us
  Pallas kernels  305 us (85%)
  matrix products  14.8 us (4%)
  between operations  14.3 us (4%)
  starting transfers between devices  8.81 us (2%)
  other arithmetic  7.49 us (2%)
  local copies, waits for them, and re-layouts  3.58 us (1%)
    pallas_call x1, Pallas kernels, dispatch(): pl.pallas_call(dispatch_kernel, name='dispatch', out_shape=(jax.ShapeDtyp...  161 us
    pallas_call x1, Pallas kernels, combine(): pl.pallas_call(combine_kernel, name='combine', out_shape=jax.ShapeDtypeSt...  145 us
    dot_general x1, matrix products, body(): jnp.dot(mixed_rows, proj_out, preferred_element_type=F32).astype(BF)  9.32 us
  transfers between devices with their start and end apart: 4, of which 1 were waited for; matrix products, arithmetic and copies ran while one was open for 1% of the time, Pallas kernels for 86%

profile of v1, /device:TPU:1, one launch (start us, length us, event | category | flops | bytes accessed | tf_op | source)
XLA Modules:
  0.0 354.8 jit_solution(12998308546180733014)
XLA Ops:
  7.2 0.0 copy-start.5
  7.2 0.0 copy-start
  7.2 0.0 all-gather.2.cloned.1.call-start
  7.2 1.6 fusion
  8.8 0.0 copy-start.3
  8.9 0.0 copy-start.2
  8.9 2.5 fusion.2
  11.4 0.0 all-gather.2.cloned.1.call-update
  11.4 0.0 reduce-scatter.2.cloned.1.call-start
  11.5 0.0 copy-done.5
  11.5 0.1 copy.27
  11.6 0.1 eq.38
  11.8 0.1 eq.42
  11.9 0.0 copy-done
  11.9 0.3 fusion.3
  12.2 0.0 copy-done.1
  12.3 0.6 reduce-window.6
  12.9 0.2 slice_reduce_fusion
  13.1 0.1 fusion.18
  13.2 0.1 reduce_sum.59
  13.4 0.1 copy.30
  13.4 0.0 copy-done.3
  13.5 0.1 pad.2.clone
  13.6 0.0 copy-done.2
  13.6 1.3 fusion.5.norm
  14.9 0.7 maximum_bitcast_fusion.meta
  15.6 160.6 %dispatch.1 = (bf16[18,4,16,512]{3,2,1,0:T(8,128)(2,1)}, bf16[4,14,16,512]{3,2,1,0:T(8,128)(2,1)}, f32[4,8,128]{2,1,0:T(8,128)}) custom-call(bf16[128,4096]{1,0:T(8,128)(2,1)} %fusion.5.norm, f32[8,128]{1,0:T(8,128)} %maximum_bitcast_fusion.meta, bf16[4096,512]{1,0:T(8,128)(2,1)} %bitcast.37, bf16[4096,512]{1,0:T(8,128)(2,1)} %bitcast.38), custom_call_target="tpu_custom_call" | custom-call | flops 99999997952 | bytes 12000000 | tf_op jit(solution)/shard_map/dispatch/pallas_call | solution.py:477
  176.2 0.0 copy-start.7
  176.2 0.0 all-gather.2.cloned.1.call-done
  176.2 0.0 copy-start.6
  176.2 4.2 %convolution_convert_fusion.1 = bf16[512,256]{1,0:T(8,128)(2,1)S(1)} fusion(bf16[512,4096]{1,0:T(8,128)(2,1)} %all-gather.2.cloned.1.call-done, bf16[4096,256]{1,0:T(8,128)(2,1)} %param.19), kind=kOutput, calls=%fused_computation.11 | convolution fusion | flops 1073872896 | bytes 6553600 | tf_op jit(solution)/shard_map/dot_general | solution.py:583
  180.5 0.0 copy-done.7
  180.5 0.4 copy-done.6
  180.9 1.2 convolution_convert_fusion.2
  182.1 0.0 copy-start.8
  182.2 2.1 collective-permute-start.1
  184.2 6.7 %collective-permute-start = (bf16[1,512]{1,0:T(2,128)(2,1)S(1)}, bf16[1,512]{1,0:T(2,128)(2,1)S(1)}, u32[]{:S(2)}, u32[]{:S(2)}) collective-permute-start(bf16[1,512]{1,0:T(2,128)(2,1)S(1)} %get-tuple-element.8), channel_id=1, source_target_pairs={{0,4},{4,8},{8,12},{12,16},{16,20},{20,24},{24,28},{28,32},{32,36}... | collective-permute-start | bytes 3080 | tf_op jit(solution)/shard_map/ppermute | solution.py:27
  190.9 0.0 copy-done.4
  190.9 0.0 collective-permute-done.1
  190.9 0.5 collective-permute-done
  191.4 0.1 pad_maximum_fusion
  191.6 0.1 convert_multiply_fusion.4
  191.6 0.0 copy-done.8
  191.6 9.3 %convolution_convert_fusion = bf16[512,4096]{1,0:T(8,128)(2,1)} fusion(bf16[256,4096]{1,0:T(8,128)(2,1)S(1)} %copy-done.8, bf16[512,4096]{1,0:T(8,128)(2,1)} %all-gather.2.cloned.1.call-done, bf16[4096,256]{1,0:T(8,128)(2,1)} %param.17, f32[514,256]{1,0:T(8,128)S(1)} %convert_multiply_fusion.4, f32[256]{0:T(256)S(1)} %bitcast.36, f32[256]{0:T(256)S(1)} %bitcast.35, ...), kind=kOutput, calls=%fused_computation | convolution fusion | flops 2150760448 | bytes 14158848 | tf_op jit(solution)/shard_map/dot_general | solution.py:594
  201.0 0.0 reduce-scatter.2.cloned.1.call-update
  201.0 144.6 %combine.1 = bf16[128,4096]{1,0:T(8,128)(2,1)} custom-call(bf16[18,4,16,512]{3,2,1,0:T(8,128)(2,1)} %get-tuple-element.5.hid_a, bf16[4,14,16,512]{3,2,1,0:T(8,128)(2,1)} %get-tuple-element.6.hid_b, f32[4,8,128]{2,1,0:T(8,128)} %get-tuple-element.7.metas, bf16[512,4096]{1,0:T(8,128)(2,1)} %bitcast.39), custom_call_target="tpu_custom_call" | custom-call | flops 99999997952 | bytes 12000000 | tf_op jit(solution)/shard_map/combine/pallas_call | solution.py:522
  345.6 0.0 reduce-scatter.2.cloned.1.call-done
  345.6 2.3 copy.36
  (18 shorter events, 0.2 us)
Async XLA Ops:
  7.2 4.3 %copy-start.5 = (s32[128,2]{0,1:T(2,128)S(1)}, s32[128,2]{0,1:T(2,128)}, u32[]{:S(2)}) copy-start(s32[128,2]{0,1:T(2,128)} %param.24) | copy-start | bytes 3076
  7.2 4.7 %copy-start = (bf16[128,4096]{1,0:T(8,128)(2,1)S(1)}, bf16[128,4096]{1,0:T(8,128)(2,1)}, u32[]{:S(2)}) copy-start(bf16[128,4096]{1,0:T(8,128)(2,1)} %param.22) | copy-start | bytes 3145732
  7.2 169.0 %all-gather.2.cloned.1.call-start = ((), (), s32[]{:S(2)}) async-start(), calls=%async_computation.1 | async-start | bytes 5242880 | tf_op jit(solution)/shard_map/all_gather | solution.py:561
  8.8 3.4 copy-start.1
  8.8 4.6 %copy-start.3 = (f32[128,2]{0,1:T(2,128)S(1)}, f32[128,2]{0,1:T(2,128)}, u32[]{:S(2)}) copy-start(f32[128,2]{0,1:T(2,128)} %param.26) | copy-start | bytes 3076
  8.9 4.7 %copy-start.2 = (f32[4096]{0:T(1024)S(1)}, f32[4096]{0:T(1024)}, u32[]{:S(2)}) copy-start(f32[4096]{0:T(1024)} %param.23) | copy-start | bytes 49156
  11.4 334.2 %reduce-scatter.2.cloned.1.call-start = ((), (), s32[]{:S(2)}) async-start(), calls=%async_computation.2 | async-start | bytes 5242880 | tf_op jit(solution)/shard_map/reduce_scatter | solution.py:593
  176.2 4.3 %copy-start.7 = (bf16[4096,256]{1,0:T(8,128)(2,1)S(1)}, bf16[4096,256]{1,0:T(8,128)(2,1)}, u32[]{:S(2)}) copy-start(bf16[4096,256]{1,0:T(8,128)(2,1)} %param.18) | copy-start | bytes 6291460
  176.2 4.7 %copy-start.6 = (bf16[512,4096]{1,0:T(8,128)(2,1)S(1)}, bf16[512,4096]{1,0:T(8,128)(2,1)}, u32[]{:S(2)}) copy-start(bf16[512,4096]{1,0:T(8,128)(2,1)} %all-gather.2.cloned.1.call-done) | copy-start | bytes 12582916
  180.9 10.0 %copy-start.4 = (bf16[3,256]{1,0:T(4,128)(2,1)S(1)}, bf16[3,256]{1,0:T(4,128)(2,1)}, u32[]{:S(2)}) copy-start(bf16[3,256]{1,0:T(4,128)(2,1)} %param.20) | copy-start | bytes 4612
  182.1 9.5 %copy-start.8 = (bf16[256,4096]{1,0:T(8,128)(2,1)S(1)}, bf16[256,4096]{1,0:T(8,128)(2,1)}, u32[]{:S(2)}) copy-start(bf16[256,4096]{1,0:T(8,128)(2,1)} %param.21) | copy-start | bytes 6291460
  182.2 8.8 %collective-permute-start.1 = (bf16[1,512]{1,0:T(2,128)(2,1)S(1)}, bf16[1,512]{1,0:T(2,128)(2,1)S(1)}, u32[]{:S(2)}, u32[]{:S(2)}) collective-permute-start(bf16[1,512]{1,0:T(2,128)(2,1)S(1)} %get-tuple-element.9), channel_id=1, source_target_pairs={{4,0},{8,4},{12,8},{16,12},{20,16},{24,20},{28,24},{32,28},{36,32}... | collective-permute-start | bytes 3080 | tf_op jit(solution)/shard_map/ppermute | solution.py:29
  184.2 7.2 %collective-permute-start = (bf16[1,512]{1,0:T(2,128)(2,1)S(1)}, bf16[1,512]{1,0:T(2,128)(2,1)S(1)}, u32[]{:S(2)}, u32[]{:S(2)}) collective-permute-start(bf16[1,512]{1,0:T(2,128)(2,1)S(1)} %get-tuple-element.8), channel_id=1, source_target_pairs={{0,4},{4,8},{8,12},{12,16},{16,20},{20,24},{24,28},{28,32},{32,36}... | collective-permute-start | bytes 3080 | tf_op jit(solution)/shard_map/ppermute | solution.py:27
Sparse Core Ops, SparseCore 0:
  11.6 77.7 all-gather.1
  201.1 83.6 reduce-scatter.1

commit v2 on v1

v2 whole, which is shorter than its diff:
```python
import jax
import jax.numpy as jnp
from jax import lax
from jax.experimental import pallas as pl
from jax.experimental.pallas import tpu as pltpu
from jax.sharding import PartitionSpec as P

GROUPS = 4
BF = jnp.bfloat16
F32 = jnp.float32
MESH = pl.DeviceIdType.MESH
SLOT = 16
NEAR = [(dz, dy, c) for dz, dy in ((0, 0), (1, 0), (3, 0), (0, 1), (0, 3), (1, 1), (3, 3), (1, 3), (3, 1)) for c in (0, 1)]
FAR = [(dz, dy, c) for dz, dy in ((2, 0), (0, 2), (2, 1), (2, 3), (1, 2), (3, 2), (2, 2)) for c in (0, 1)]
NA = len(NEAR)
NB = len(FAR)
NC = 4
PER = 3


def place(x, r):
    return (x + (3 * ((r * (r + 1)) // 2)) % 4) % 4


def peer(me, offset, sign):
    z, y, c = me // 8, (me // 2) % 4, me % 2
    dz, dy, dc = offset
    return (((z + sign * dz + 4) % 4) * 4 + (y + sign * dy + 4) % 4) * 2 + (c + dc) % 2


def greet(me, x):
    barrier = pltpu.get_barrier_semaphore()
    for offset in NEAR[1:] + FAR:
        pl.semaphore_signal(barrier, inc=1, device_id=(peer(me, offset, 1), x), device_id_type=MESH)
    pl.semaphore_signal(barrier, inc=1, device_id=(me, (x + 1) % 4), device_id_type=MESH)
    pl.semaphore_signal(barrier, inc=1, device_id=(me, (x + 3) % 4), device_id_type=MESH)
    pl.semaphore_wait(barrier, NA - 1 + NB + 2)


def remote(src, dst, send, recv, ep, tp):
    return pltpu.make_async_remote_copy(
        src_ref=src, dst_ref=dst, send_sem=send, recv_sem=recv, device_id=(ep, tp), device_id_type=MESH
    )


def slot_rows(base, rows, meta, hit0, hit1):
    want = lax.broadcasted_iota(jnp.int32, (rows, meta.shape[1]), 0) + base
    want = want.astype(F32)
    return jnp.where(meta[0:1] == want, hit0, 0.0) + jnp.where(meta[1:2] == want, hit1, 0.0)


def normed(raw, gain, into, width):
    step = 16
    cw = into.shape[3]

    def one(t, _):
        span = pl.ds(pl.multiple_of(t * step, step), step)
        values = raw[span, :].astype(F32)
        scale = lax.rsqrt(jnp.sum(values * values, axis=1, keepdims=True) * (1.0 / width) + 1e-06)
        values = (values * scale * gain[...]).astype(BF)
        for c in range(NC):
            into[c, 0, span, :] = values[:, c * cw:(c + 1) * cw]
        return 0

    lax.fori_loop(0, raw.shape[0] // step, one, 0)


def dispatch_kernel(
    moe_hbm, moe_gain, meta, gate_hbm, up_hbm, mix_hbm, mix_gain, projb_hbm, projc_hbm, projh_hbm, taps,
    hid_a, hid_b, metas_out, mixed,
    moe_raw, mix_raw, tok, mix, metas, oh_a, oh_b, out_a, out_b, recv_a, recv_b, gate_w, up_w, proj_w,
    bcc_g, bcc_u, cin, gate_b,
    tok_s, tok_r, tokf_s, tokf_r, mx_s, mx_r, mxf_s, mxf_r, b_s, b_r, bx_s, bx_r, bf_s, bf_r, a_s, a_r,
    meta_s, meta_r, halo_s, halo_r, w_sem,
):
    me = lax.axis_index("ep")
    x = lax.axis_index("tp")
    right, left = (x + 1) % 4, (x + 3) % 4
    rows, cw = tok.shape[2], tok.shape[3]
    width = NC * cw
    half = rows // 2
    hb = NB // 2
    chan = gate_b.shape[1]
    moe_in = pltpu.make_async_copy(moe_hbm, moe_raw, w_sem.at[0])
    mix_in = pltpu.make_async_copy(mix_hbm, mix_raw, w_sem.at[1])
    loads = [
        pltpu.make_async_copy(gate_hbm, gate_w, w_sem.at[2]),
        pltpu.make_async_copy(up_hbm, up_w, w_sem.at[3]),
        pltpu.make_async_copy(projb_hbm, proj_w.at[0], w_sem.at[4]),
        pltpu.make_async_copy(projc_hbm, proj_w.at[1], w_sem.at[5]),
        pltpu.make_async_copy(projh_hbm, proj_w.at[2], w_sem.at[6]),
    ]
    moe_in.start()
    mix_in.start()
    for load in loads:
        load.start()
    greet(me, x)

    meta_right = remote(meta, metas.at[1], meta_s.at[0], meta_r.at[0], me, right)
    meta_left = remote(meta, metas.at[2], meta_s.at[1], meta_r.at[1], me, left)
    meta_on = remote(metas.at[1], metas.at[3], meta_s.at[2], meta_r.at[2], me, right)
    meta_right.start()
    meta_left.start()

    def ring(buf, one_s, one_r, two_s, two_r):
        size = buf.shape[2] // 2
        lo, hi = pl.ds(0, size), pl.ds(size, size)
        return (
            lambda c: remote(buf.at[c, 0], buf.at[c, 1], one_s.at[c, 0], one_r.at[c, 0], me, right),
            lambda c: remote(buf.at[c, 0], buf.at[c, 2], one_s.at[c, 1], one_r.at[c, 1], me, left),
            lambda c: remote(buf.at[c, 1, lo], buf.at[c, 3, lo], two_s.at[c, 0], two_r.at[c, 0], me, right),
            lambda c: remote(buf.at[c, 2, hi], buf.at[c, 3, hi], two_s.at[c, 1], two_r.at[c, 1], me, left),
        )

    tok_right, tok_left, tok_on_right, tok_on_left = ring(tok, tok_s, tok_r, tokf_s, tokf_r)
    mix_right, mix_left, mix_on_right, mix_on_left = ring(mix, mx_s, mx_r, mxf_s, mxf_r)
    b_right, b_left, b_on_right, b_on_left = ring(recv_b, bx_s, bx_r, bf_s, bf_r)

    def a_all(c):
        span = pl.ds(1, NA - 1)
        return remote(out_a.at[c, span], recv_a.at[c, span], a_s.at[c], a_r.at[c], me, right)

    def b_all(c):
        return remote(out_b.at[c], recv_b.at[c, 0], b_s.at[c], b_r.at[c], me, right)

    moe_in.wait()
    normed(moe_raw, moe_gain, tok, width)

    def first(c, _):
        tok_right(c).start()
        tok_left(c).start()
        return 0

    lax.fori_loop(0, NC, first, 0)

    own = meta[...]
    for o in range(NB):
        oh_b[o] = slot_rows(peer(me, FAR[o], 1) * SLOT, SLOT, own, 1.0, 1.0).astype(BF)

    def second(c, _):
        picked = jnp.dot(oh_b[...].reshape(NB * SLOT, rows), tok[c, 0], preferred_element_type=F32)
        out_b[c] = picked.astype(BF).reshape(NB, SLOT, cw)
        for o in range(NB):
            remote(out_b.at[c, o], recv_b.at[c, 0, o], b_s.at[c], b_r.at[c], peer(me, FAR[o], 1), x).start()
        return 0

    lax.fori_loop(0, NC, second, 0)

    meta_right.wait()
    meta_on.start()
    meta_left.wait()
    meta_on.wait()
    metas[0] = own
    metas_out[...] = metas[...]
    for o in range(NA):
        base = peer(me, NEAR[o], 1) * SLOT
        for r in range(4):
            oh_a[r, o] = slot_rows(base, SLOT, metas_out[r], 1.0, 1.0).astype(BF)
    mix_in.wait()
    normed(mix_raw, mix_gain, mix, width)

    def third(c, _):
        def pick(r):
            picked = jnp.dot(oh_a[r].reshape(NA * SLOT, rows), tok[c, r], preferred_element_type=F32).astype(BF)
            picked = picked.reshape(NA, SLOT, cw)
            recv_a[c, 0, r] = picked[0]
            out_a[c, 1:, r] = picked[1:]

        pick(0)
        tok_right(c).wait_recv()
        tok_on_right(c).start()
        tok_left(c).wait_recv()
        tok_on_left(c).start()
        mix_right(c).start()
        mix_left(c).start()
        pick(1)
        pick(2)
        tok_on_right(c).wait_recv()
        tok_on_left(c).wait_recv()
        pick(3)
        for o in range(1, NA):
            remote(out_a.at[c, o], recv_a.at[c, o], a_s.at[c], a_r.at[c], peer(me, NEAR[o], 1), x).start()
        b_all(c).wait_recv()
        b_right(c).start()
        b_left(c).start()
        return 0

    lax.fori_loop(0, NC, third, 0)

    def fourth(c, _):
        mix_right(c).wait_recv()
        mix_on_right(c).start()
        mix_left(c).wait_recv()
        mix_on_left(c).start()
        b_right(c).wait_recv()
        b_on_right(c).start()
        b_left(c).wait_recv()
        b_on_left(c).start()
        return 0

    lax.fori_loop(0, NC, fourth, 0)
    for load in loads:
        load.wait()

    def finish(gate_val, up_val):
        return (gate_val / (1.0 + jnp.exp(-gate_val)) * up_val).astype(BF)

    def chunk_dots(values, mats, c):
        return [jnp.dot(values, mat[c * cw:(c + 1) * cw], preferred_element_type=F32) for mat in mats]

    for c in range(NC):
        a_all(c).wait_recv()

    def step_a(t, _):
        total = None
        for c in range(NC):
            values = recv_a[c, pl.ds(t * PER, PER)].reshape(PER * 4 * SLOT, cw)
            parts = chunk_dots(values, (gate_w, up_w), c)
            total = parts if total is None else [one + two for one, two in zip(total, parts)]
        hid_a[pl.ds(t * PER, PER)] = finish(*total).reshape(PER, 4, SLOT, gate_w.shape[1])
        return 0

    lax.fori_loop(0, NA // PER, step_a, 0)

    for c in range(NC):
        mix_on_right(c).wait_recv()
        mix_on_left(c).wait_recv()

    def project(r, _):
        start = pl.multiple_of(place(x, r) * rows, rows)
        total = None
        for c in range(NC):
            parts = chunk_dots(mix[c, r], [proj_w.at[n] for n in range(3)], c)
            total = parts if total is None else [one + two for one, two in zip(total, parts)]
        gate_b[pl.ds(start, rows)] = total[0].astype(BF)
        cin[pl.ds(start + 8, rows)] = total[1].astype(BF).astype(F32) * total[2].astype(BF).astype(F32)
        return 0

    lax.fori_loop(0, 4, project, 0)
    last = 4 * rows
    halo_next = remote(cin.at[pl.ds(last, 8)], cin.at[pl.ds(0, 8)], halo_s.at[0], halo_r.at[0], (me + 1) % 32, x)
    halo_prev = remote(cin.at[pl.ds(8, 8)], cin.at[pl.ds(last + 8, 8)], halo_s.at[1], halo_r.at[1], (me + 31) % 32, x)
    halo_next.start()
    halo_prev.start()

    for c in range(NC):
        b_on_right(c).wait_recv()
        b_on_left(c).wait_recv()

        def step_b(r, _, c=c):
            g, u = chunk_dots(recv_b[c, r].reshape(NB * SLOT, cw), (gate_w, up_w), c)
            if c > 0:
                g = g + bcc_g[r]
                u = u + bcc_u[r]
            if c < NC - 1:
                bcc_g[r] = g
                bcc_u[r] = u
            else:
                hid_b[r] = finish(g, u).reshape(NB, SLOT, g.shape[1])
            return 0

        lax.fori_loop(0, 4, step_b, 0)

    halo_next.wait()
    halo_prev.wait()
    cin[0:8] = cin[0:8] * jnp.where(me > 0, 1.0, 0.0)
    cin[last + 8:last + 16] = cin[last + 8:last + 16] * jnp.where(me < 31, 1.0, 0.0)
    tap = taps[...].astype(F32)
    conv = tap[0:1] * cin[7:last + 7] + tap[1:2] * cin[8:last + 8] + tap[2:3] * cin[9:last + 9]
    mixed[...] = (gate_b[...].astype(F32) * conv).astype(BF)

    def drain(c, _):
        for copy in (
            tok_right, tok_left, tok_on_right, tok_on_left, mix_right, mix_left, mix_on_right, mix_on_left,
            b_all, b_right, b_left, b_on_right, b_on_left, a_all,
        ):
            copy(c).wait_send()
        return 0

    lax.fori_loop(0, NC, drain, 0)


def combine_kernel(
    hid_a, hid_b, metas, down_hbm, mixed, proj_hbm,
    out, mix_out,
    down_w, proj_w, p_a, p_b, bh_in, bf_in, sum_b, ret_a, ret_b, w_a, w_b, p_t, th_in, tf_in, p_m, mh_in, mf_in,
    bh_s, bh_r, bf_s, bf_r, b_s, b_r, a_s, a_r, th_s, th_r, tf_s, tf_r, mh_s, mh_r, mf_s, mf_r, w_sem,
):
    me = lax.axis_index("ep")
    x = lax.axis_index("tp")
    right, left = (x + 1) % 4, (x + 3) % 4
    cw = p_a.shape[4]
    rows = p_t.shape[2]
    half = rows // 2
    hb = NB // 2
    down_in = pltpu.make_async_copy(down_hbm, down_w, w_sem.at[0])
    proj_in = pltpu.make_async_copy(proj_hbm, proj_w, w_sem.at[1])
    down_in.start()
    proj_in.start()
    greet(me, x)

    def cols(c):
        return pl.ds(pl.multiple_of(c * cw, cw), cw)

    def ring(buf, halves, wholes, one_s, one_r, two_s, two_r):
        size = buf.shape[2] // 2
        top = buf.shape[1] - 1
        return (
            lambda c: remote(buf.at[c, top, pl.ds(0, size)], halves.at[c, 0], one_s.at[c, 0], one_r.at[c, 0], me, right),
            lambda c: remote(buf.at[c, top, pl.ds(size, size)], halves.at[c, 1], one_s.at[c, 1], one_r.at[c, 1], me, left),
            lambda c: remote(buf.at[c, top - 1], wholes.at[c, 0], two_s.at[c, 0], two_r.at[c, 0], me, right),
            lambda c: remote(buf.at[c, top - 2], wholes.at[c, 1], two_s.at[c, 1], two_r.at[c, 1], me, left),
        )

    b_ring = ring(p_b, bh_in, bf_in, bh_s, bh_r, bf_s, bf_r)
    t_ring = ring(p_t, th_in, tf_in, th_s, th_r, tf_s, tf_r)
    m_ring = ring(p_m, mh_in, mf_in, mh_s, mh_r, mf_s, mf_r)

    def open_ring(copies, c):
        copies[0](c).start()
        copies[1](c).start()

    def pass_on(copies, buf, halves, c):
        size = buf.shape[2] // 2
        top = buf.shape[1] - 1
        copies[0](c).wait_recv()
        buf[c, top - 1, :size] = (buf[c, top - 1, :size].astype(F32) + halves[c, 0].astype(F32)).astype(BF)
        copies[2](c).start()
        copies[1](c).wait_recv()
        buf[c, top - 2, size:] = (buf[c, top - 2, size:].astype(F32) + halves[c, 1].astype(F32)).astype(BF)
        copies[3](c).start()

    def arrivals(copies, wholes, c):
        copies[2](c).wait_recv()
        copies[3](c).wait_recv()
        return wholes[c, 0].astype(F32) + wholes[c, 1].astype(F32)

    def a_all(c):
        span = pl.ds(1, NA - 1)
        return remote(p_a.at[c, span], ret_a.at[c, span], a_s.at[c], a_r.at[c], me, right)

    def b_all(c):
        return remote(sum_b.at[c], ret_b.at[c], b_s.at[c], b_r.at[c], me, right)

    down_in.wait()

    def first(c, _):
        def one(r, _):
            part = jnp.dot(hid_b[r].reshape(NB * SLOT, hid_b.shape[3]), down_w[:, cols(c)], preferred_element_type=F32)
            p_b[c, r] = part.astype(BF).reshape(NB, SLOT, cw)
            return 0

        lax.fori_loop(0, 4, one, 0)
        open_ring(b_ring, c)
        return 0

    lax.fori_loop(0, NC, first, 0)

    def second(c, _):
        def one(t, _):
            span = pl.ds(t * PER, PER)
            values = hid_a[span].reshape(PER * 4 * SLOT, hid_a.shape[3])
            part = jnp.dot(values, down_w[:, cols(c)], preferred_element_type=F32)
            p_a[c, span] = part.astype(BF).reshape(PER, 4, SLOT, cw)
            return 0

        lax.fori_loop(0, NA // PER, one, 0)
        for o in range(1, NA):
            remote(p_a.at[c, o], ret_a.at[c, o], a_s.at[c], a_r.at[c], peer(me, NEAR[o], -1), x).start()
        ret_a[c, 0] = p_a[c, 0]
        pass_on(b_ring, p_b, bh_in, c)
        return 0

    lax.fori_loop(0, NC, second, 0)
    proj_in.wait()

    def mixer(c, _):
        def one(r, _):
            values = mixed[pl.ds(pl.multiple_of(place(x, r) * rows, rows), rows)]
            p_m[c, r] = jnp.dot(values, proj_w[:, cols(c)], preferred_element_type=F32).astype(BF)
            return 0

        lax.fori_loop(0, 4, one, 0)
        open_ring(m_ring, c)
        return 0

    lax.fori_loop(0, NC, mixer, 0)

    for o in range(NA):
        base = peer(me, NEAR[o], 1) * SLOT
        for r in range(4):
            meta = metas[r]
            w_a[r, o] = slot_rows(base, SLOT, meta, meta[2:3], meta[3:4]).astype(BF)
    for o in range(NB):
        meta = metas[0]
        w_b[o] = slot_rows(peer(me, FAR[o], 1) * SLOT, SLOT, meta, meta[2:3], meta[3:4]).astype(BF)

    def third(c, _):
        sum_b[c] = (p_b[c, 0].astype(F32) + arrivals(b_ring, bf_in, c)).astype(BF)
        for o in range(NB):
            remote(sum_b.at[c, o], ret_b.at[c, o], b_s.at[c], b_r.at[c], peer(me, FAR[o], -1), x).start()
        pass_on(m_ring, p_m, mh_in, c)
        return 0

    lax.fori_loop(0, NC, third, 0)
    over_rows = (((0,), (0,)), ((), ()))

    def weighed(r, c):
        values = ret_a[c, :, r].reshape(NA * SLOT, cw)
        return lax.dot_general(w_a[r].reshape(NA * SLOT, rows), values, over_rows, preferred_element_type=F32)

    def fourth(c, _):
        a_all(c).wait_recv()
        p_t[c, 2] = weighed(3, c).astype(BF)
        open_ring(t_ring, c)
        p_t[c, 0] = weighed(1, c).astype(BF)
        p_t[c, 1] = weighed(2, c).astype(BF)
        pass_on(t_ring, p_t, th_in, c)
        return 0

    lax.fori_loop(0, NC, fourth, 0)

    def fifth(c, _):
        mix_out[:, cols(c)] = (p_m[c, 0].astype(F32) + arrivals(m_ring, mf_in, c)).astype(BF)
        return 0

    lax.fori_loop(0, NC, fifth, 0)

    def sixth(c, _):
        b_all(c).wait_recv()
        values = ret_b[c].reshape(NB * SLOT, cw)
        total = weighed(0, c) + lax.dot_general(
            w_b[...].reshape(NB * SLOT, rows), values, over_rows, preferred_element_type=F32
        )
        out[:, cols(c)] = (total + arrivals(t_ring, tf_in, c)).astype(BF)
        return 0

    lax.fori_loop(0, NC, sixth, 0)

    def drain(c, _):
        for copy in b_ring + t_ring + m_ring + (a_all, b_all):
            copy(c).wait_send()
        return 0

    lax.fori_loop(0, NC, drain, 0)


VM = pltpu.VMEM
DMA = pltpu.SemaphoreType.DMA
PARAMS = dict(has_side_effects=True, vmem_limit_bytes=64 * 1024 * 1024 - 65536)
COST = pl.CostEstimate(flops=100_000_000_000, bytes_accessed=12_000_000, transcendentals=0)


def specs(places):
    vmem = pl.BlockSpec(memory_space=VM)
    anywhere = pl.BlockSpec(memory_space=pl.ANY)
    return [vmem if place == "v" else anywhere for place in places]


def dispatch(moe_in, moe_gain, meta, gate_mat, up_mat, mix_in, mix_gain, proj_b, proj_c, proj_h, taps):
    rows, width = moe_in.shape
    hidden = gate_mat.shape[1]
    chan = proj_b.shape[1]
    cw = width // NC
    pair = DMA((NC, 2))
    single = DMA((NC,))
    return pl.pallas_call(
        dispatch_kernel,
        name="dispatch",
        out_shape=(
            jax.ShapeDtypeStruct((NA, 4, SLOT, hidden), BF),
            jax.ShapeDtypeStruct((4, NB, SLOT, hidden), BF),
            jax.ShapeDtypeStruct((4,) + meta.shape, F32),
            jax.ShapeDtypeStruct((4 * rows, chan), BF),
        ),
        in_specs=specs("avvaaavaaav"),
        out_specs=tuple(specs("vvvv")),
        scratch_shapes=[
            VM((rows, width), BF),
            VM((rows, width), BF),
            VM((NC, 4, rows, cw), BF),
            VM((NC, 4, rows, cw), BF),
            VM((4,) + meta.shape, F32),
            VM((4, NA, SLOT, rows), BF),
            VM((NB, SLOT, rows), BF),
            VM((NC, NA, 4, SLOT, cw), BF),
            VM((NC, NB, SLOT, cw), BF),
            VM((NC, NA, 4, SLOT, cw), BF),
            VM((NC, 4, NB, SLOT, cw), BF),
            VM((width, hidden), BF),
            VM((width, hidden), BF),
            VM((3, width, chan), BF),
            VM((4, NB * SLOT, hidden), F32),
            VM((4, NB * SLOT, hidden), F32),
            VM((4 * rows + 16, chan), F32),
            VM((4 * rows, chan), BF),
            pair, pair, pair, pair, pair, pair, pair, pair, single, single, pair, pair, pair, pair, single, single,
            DMA((3,)), DMA((3,)), DMA((2,)), DMA((2,)), DMA((7,)),
        ],
        compiler_params=pltpu.CompilerParams(collective_id=0, **PARAMS),
        cost_estimate=COST,
    )(moe_in, moe_gain, meta, gate_mat, up_mat, mix_in, mix_gain, proj_b, proj_c, proj_h, taps)


def combine(hid_a, hid_b, metas, down_mat, mixed, proj_out):
    rows = metas.shape[2]
    hidden, width = down_mat.shape
    chan = proj_out.shape[0]
    cw = width // NC
    hb = NB // 2
    pair = DMA((NC, 2))
    single = DMA((NC,))
    return pl.pallas_call(
        combine_kernel,
        name="combine",
        out_shape=(jax.ShapeDtypeStruct((rows, width), BF), jax.ShapeDtypeStruct((rows, width), BF)),
        in_specs=specs("vvvava"),
        out_specs=tuple(specs("vv")),
        scratch_shapes=[
            VM((hidden, width), BF),
            VM((chan, width), BF),
            VM((NC, NA, 4, SLOT, cw), BF),
            VM((NC, 4, NB, SLOT, cw), BF),
            VM((NC, 2, hb, SLOT, cw), BF),
            VM((NC, 2, NB, SLOT, cw), BF),
            VM((NC, NB, SLOT, cw), BF),
            VM((NC, NA, 4, SLOT, cw), BF),
            VM((NC, NB, SLOT, cw), BF),
            VM((4, NA, SLOT, rows), BF),
            VM((NB, SLOT, rows), BF),
            VM((NC, 3, rows, cw), BF),
            VM((NC, 2, rows // 2, cw), BF),
            VM((NC, 2, rows, cw), BF),
            VM((NC, 4, rows, cw), BF),
            VM((NC, 2, rows // 2, cw), BF),
            VM((NC, 2, rows, cw), BF),
            pair, pair, pair, pair, single, single, single, single,
            pair, pair, pair, pair, pair, pair, pair, pair, DMA((2,)),
        ],
        compiler_params=pltpu.CompilerParams(collective_id=1, **PARAMS),
        cost_estimate=COST,
    )(hid_a, hid_b, metas, down_mat, mixed, proj_out)


def body(
    mix_in, mix_gain, proj_b, proj_c, proj_h, conv_taps, proj_out,
    moe_in, moe_gain, routes, group_logits, pair_logits, expert_gate, expert_up, expert_down,
):
    local_rows, top_count = routes.shape
    experts_all = lax.axis_size("ep")
    flat_routes = routes.reshape(-1)
    route_hits = (flat_routes[:, None] == jnp.arange(experts_all, dtype=jnp.int32)[None, :]).astype(jnp.int32)
    route_ranks = jnp.sum((jnp.cumsum(route_hits, axis=0) - route_hits) * route_hits, axis=1)
    slot_ids = (flat_routes * SLOT + route_ranks).reshape(local_rows, top_count)
    group_prob = jax.nn.softmax(group_logits, axis=-1)
    member = routes // (experts_all // GROUPS)
    picked_prob = jnp.sum(
        group_prob[:, None, :]
        * (member[:, :, None] == jnp.arange(GROUPS, dtype=jnp.int32)[None, None, :]).astype(F32),
        axis=-1,
    )
    weight = picked_prob * jax.nn.softmax(pair_logits, axis=-1)
    meta = jnp.concatenate([slot_ids.astype(F32), weight, jnp.zeros((local_rows, 4), F32)], axis=1).T

    hid_a, hid_b, metas, mixed = dispatch(
        moe_in, moe_gain[None, :], meta, expert_gate[0], expert_up[0],
        mix_in, mix_gain[None, :], proj_b, proj_c, proj_h, conv_taps,
    )
    moe_out, mix_out = combine(hid_a, hid_b, metas, expert_down[0], mixed, proj_out)
    return (mix_out, moe_out)


def solution(mesh):
    in_specs = (
        P(("ep", "tp"), None), P(), P(None, "tp"), P(None, "tp"), P(None, "tp"), P(None, "tp"), P("tp", None),
        P(("ep", "tp"), None), P(), P(("ep", "tp"), None), P(("ep", "tp"), None), P(("ep", "tp"), None),
        P("ep", None, "tp"), P("ep", None, "tp"), P("ep", "tp", None),
    )
    out_specs = (P(("ep", "tp"), None), P(("ep", "tp"), None))
    return jax.shard_map(body, mesh=mesh, in_specs=in_specs, out_specs=out_specs, check_vma=False)
```

time: 358 us -> 309 us (0.86)
  matrix products: 14.8 us -> 0 us
  between operations: 14.3 us -> 0.69 us
  Pallas kernels: 305 us -> 295 us
  starting transfers between devices: 8.81 us -> 0 us
    dot_general x3 -> x0, matrix products: 14.8 us -> none  [the longest x1 9.32 us: body(): jnp.dot(mixed_rows, proj_out, preferred_element_type=F32).astype(BF)]
    ppermute x2 -> x0, starting transfers between devices: 8.73 us -> none  [the longest x1 6.67 us: with_halo(): lax.ppermute(tail, axis, [(i, (i + 1) % count) for i in range(ends)])]
    pallas_call x1, Pallas kernels: 161 us -> 154 us  [dispatch(): pl.pallas_call(dispatch_kernel, name='dispatch', out_shape=(jax.ShapeDtyp...]
    pallas_call x1, Pallas kernels: 145 us -> 140 us  [combine(): pl.pallas_call(combine_kernel, name='combine', out_shape=(jax.ShapeDtypeS...]
    convert_element_type x2 -> x0, other arithmetic: 3.84 us -> none  [rms_scaled(): return (scaled * gain_vec).astype(BF)]
  transfers between devices with their start and end apart: 4 -> 0, of which waited for: 1 -> 0; matrix products, arithmetic and copies ran while one was open for 1% -> 0% of each run, Pallas kernels for 86% -> 0%
where the time goes in v2:
time: 309 us; the launch traced here: 306 us
  Pallas kernels  295 us (95%)
  other arithmetic  6.31 us (2%)
  local copies, waits for them, and re-layouts  4.88 us (2%)
    pallas_call x1, Pallas kernels, dispatch(): pl.pallas_call(dispatch_kernel, name='dispatch', out_shape=(jax.ShapeDtyp...  154 us
    pallas_call x1, Pallas kernels, combine(): pl.pallas_call(combine_kernel, name='combine', out_shape=(jax.ShapeDtypeS...  140 us

profile of v2, /device:TPU:1, one launch (start us, length us, event | category | flops | bytes accessed | tf_op | source)
XLA Modules:
  0.0 306.4 jit_solution(14536931660002787736)
XLA Ops:
  0.6 0.7 reduce_max.18
  1.3 0.7 reduce_max.19
  2.0 0.7 fusion.6
  2.7 0.7 fusion.5
  3.4 0.1 pad.2.clone
  3.5 0.7 fusion.4
  4.2 0.8 copy.25
  5.0 0.1 eq.42
  5.1 0.1 eq.38
  5.3 0.6 reduce-window.6
  5.9 0.2 slice_reduce_fusion
  6.1 0.1 fusion.2
  6.2 0.1 reduce_sum.39
  6.4 0.1 copy.28
  6.4 0.7 add_convert_fusion
  7.2 0.7 divide_multiply_fusion
  7.8 0.7 maximum_bitcast_fusion.meta
  8.5 154.3 %dispatch.1 = (bf16[18,4,16,512]{3,2,1,0:T(8,128)(2,1)}, bf16[4,14,16,512]{3,2,1,0:T(8,128)(2,1)}, f32[4,8,128]{2,1,0:T(8,128)}, bf16[512,256]{1,0:T(8,128)(2,1)}) custom-call(bf16[128,4096]{1,0:T(8,128)(2,1)} %moe_hbm.1, f32[1,4096]{1,0:T(1,128)} %bitcast.29, f32[8,128]{1,0:T(8,128)} %maximum_bitcast_fusion.meta, bf16[4096,512]{1,0:T(8,128)(2,1)} %bitcast.26, ...), custom_call_target="tpu_custom_call" | custom-call | flops 99999997952 | bytes 12000000 | tf_op jit(solution)/shard_map/dispatch/pallas_call | solution.py:467
  162.8 140.2 %combine.1 = (bf16[128,4096]{1,0:T(8,128)(2,1)}, bf16[128,4096]{1,0:T(8,128)(2,1)}) custom-call(bf16[18,4,16,512]{3,2,1,0:T(8,128)(2,1)} %get-tuple-element.8.hid_a, bf16[4,14,16,512]{3,2,1,0:T(8,128)(2,1)} %get-tuple-element.9.hid_b, f32[4,8,128]{2,1,0:T(8,128)} %get-tuple-element.10.metas, bf16[512,4096]{1,0:T(8,128)(2,1)} %bitcast.28, ...), custom_call_target="tpu_custom_call" | custom-call | flops 99999997952 | bytes 12000000 | tf_op jit(solution)/shard_map/combine/pallas_call | solution.py:513
  303.0 0.0 copy-start
  303.0 2.4 copy.33
  305.4 0.0 copy-done
  305.4 1.0 copy.34
  (5 shorter events, 0.1 us)
Async XLA Ops:
  303.0 2.4 copy-start

commit v3 on v2

--- a/solution.py
+++ b/solution.py
@@ -10,12 +10,16 @@
 F32 = jnp.float32
 MESH = pl.DeviceIdType.MESH
 SLOT = 16
-NEAR = [(dz, dy, c) for dz, dy in ((0, 0), (1, 0), (3, 0), (0, 1), (0, 3), (1, 1), (3, 3), (1, 3), (3, 1)) for c in (0, 1)]
-FAR = [(dz, dy, c) for dz, dy in ((2, 0), (0, 2), (2, 1), (2, 3), (1, 2), (3, 2), (2, 2)) for c in (0, 1)]
+def both(*chips):
+    return [(dz, dy, c) for dz, dy in chips for c in (0, 1)]
+
+
+NEAR = both((0, 0), (1, 0), (3, 0), (0, 1), (0, 3)) + [(2, 0, 0), (0, 2, 0)] + both((1, 1), (3, 3), (1, 3), (3, 1))
+FAR = [(2, 0, 1), (0, 2, 1)] + both((2, 1), (2, 3), (1, 2), (3, 2), (2, 2))
 NA = len(NEAR)
 NB = len(FAR)
 NC = 4
-PER = 3
+PER = 4
 
 
 def place(x, r):
@@ -34,7 +38,7 @@
         pl.semaphore_signal(barrier, inc=1, device_id=(peer(me, offset, 1), x), device_id_type=MESH)
     pl.semaphore_signal(barrier, inc=1, device_id=(me, (x + 1) % 4), device_id_type=MESH)
     pl.semaphore_signal(barrier, inc=1, device_id=(me, (x + 3) % 4), device_id_type=MESH)
-    pl.semaphore_wait(barrier, NA - 1 + NB + 2)
+    return lambda: pl.semaphore_wait(barrier, NA - 1 + NB + 2)
 
 
 def remote(src, dst, send, recv, ep, tp):
@@ -47,6 +51,32 @@
     want = lax.broadcasted_iota(jnp.int32, (rows, meta.shape[1]), 0) + base
     want = want.astype(F32)
     return jnp.where(meta[0:1] == want, hit0, 0.0) + jnp.where(meta[1:2] == want, hit1, 0.0)
+
+
+def routing(routes, group_logits, pair_logits):
+    count = routes.shape[1]
+    r0, r1 = routes[0:1], routes[1:2]
+    expert = lax.broadcasted_iota(jnp.int32, (32, count), 0)
+    hit0, hit1 = jnp.where(expert == r0, 1.0, 0.0), jnp.where(expert == r1, 1.0, 0.0)
+    earlier = lax.broadcasted_iota(jnp.int32, (count, count), 0) < lax.broadcasted_iota(jnp.int32, (count, count), 1)
+    before = jnp.dot((hit0 + hit1).astype(BF), jnp.where(earlier, 1.0, 0.0).astype(BF), preferred_element_type=F32)
+
+    def share(logits):
+        grown = jnp.exp(logits - jnp.max(logits, axis=0, keepdims=True))
+        return grown / jnp.sum(grown, axis=0, keepdims=True)
+
+    group, pair = share(group_logits), share(pair_logits)
+
+    def one(route, hit, k):
+        slot = route.astype(F32) * SLOT + jnp.sum(before * hit, axis=0, keepdims=True)
+        member = sum(
+            group[g:g + 1] * jnp.where(jnp.logical_and(route >= 8 * g, route < 8 * g + 8), 1.0, 0.0) for g in range(GROUPS)
+        )
+        return slot, member * pair[k:k + 1]
+
+    slot0, weight0 = one(r0, hit0, 0)
+    slot1, weight1 = one(r1, hit1, 1)
+    return jnp.concatenate([slot0, slot1, weight0, weight1, jnp.zeros((4, count), F32)], axis=0)
 
 
 def normed(raw, gain, into, width):
@@ -66,10 +96,10 @@
 
 
 def dispatch_kernel(
-    moe_hbm, moe_gain, meta, gate_hbm, up_hbm, mix_hbm, mix_gain, projb_hbm, projc_hbm, projh_hbm, taps,
+    moe_hbm, moe_gain, routes, group_logits, pair_logits, gate_hbm, up_hbm, mix_hbm, mix_gain, projb_hbm, projc_hbm, projh_hbm, taps,
     hid_a, hid_b, metas_out, mixed,
-    moe_raw, mix_raw, tok, mix, metas, oh_a, oh_b, out_a, out_b, recv_a, recv_b, gate_w, up_w, proj_w,
-    bcc_g, bcc_u, cin, gate_b,
+    raw, tok, mix, metas, oh_a, oh_b, out_a, out_b, recv_a, recv_b, gate_w, up_w, proj_w,
+    acc_g, acc_u, bcc_g, bcc_u, cin, gate_b,
     tok_s, tok_r, tokf_s, tokf_r, mx_s, mx_r, mxf_s, mxf_r, b_s, b_r, bx_s, bx_r, bf_s, bf_r, a_s, a_r,
     meta_s, meta_r, halo_s, halo_r, w_sem,
 ):
@@ -81,8 +111,8 @@
     half = rows // 2
     hb = NB // 2
     chan = gate_b.shape[1]
-    moe_in = pltpu.make_async_copy(moe_hbm, moe_raw, w_sem.at[0])
-    mix_in = pltpu.make_async_copy(mix_hbm, mix_raw, w_sem.at[1])
+    moe_in = pltpu.make_async_copy(moe_hbm, raw, w_sem.at[0])
+    mix_in = pltpu.make_async_copy(mix_hbm, raw, w_sem.at[1])
     loads = [
         pltpu.make_async_copy(gate_hbm, gate_w, w_sem.at[2]),
         pltpu.make_async_copy(up_hbm, up_w, w_sem.at[3]),
@@ -91,13 +121,17 @@
         pltpu.make_async_copy(projh_hbm, proj_w.at[2], w_sem.at[6]),
     ]
     moe_in.start()
-    mix_in.start()
+    everyone_in = greet(me, x)
     for load in loads:
         load.start()
-    greet(me, x)
-
-    meta_right = remote(meta, metas.at[1], meta_s.at[0], meta_r.at[0], me, right)
-    meta_left = remote(meta, metas.at[2], meta_s.at[1], meta_r.at[1], me, left)
+    metas[0] = routing(routes[...], group_logits[...], pair_logits[...])
+    moe_in.wait()
+    normed(raw, moe_gain, tok, width)
+    mix_in.start()
+    everyone_in()
+
+    meta_right = remote(metas.at[0], metas.at[1], meta_s.at[0], meta_r.at[0], me, right)
+    meta_left = remote(metas.at[0], metas.at[2], meta_s.at[1], meta_r.at[1], me, left)
     meta_on = remote(metas.at[1], metas.at[3], meta_s.at[2], meta_r.at[2], me, right)
     meta_right.start()
     meta_left.start()
@@ -123,9 +157,6 @@
     def b_all(c):
         return remote(out_b.at[c], recv_b.at[c, 0], b_s.at[c], b_r.at[c], me, right)
 
-    moe_in.wait()
-    normed(moe_raw, moe_gain, tok, width)
-
     def first(c, _):
         tok_right(c).start()
         tok_left(c).start()
@@ -133,7 +164,7 @@
 
     lax.fori_loop(0, NC, first, 0)
 
-    own = meta[...]
+    own = metas[0]
     for o in range(NB):
         oh_b[o] = slot_rows(peer(me, FAR[o], 1) * SLOT, SLOT, own, 1.0, 1.0).astype(BF)
 
@@ -150,55 +181,72 @@
     meta_on.start()
     meta_left.wait()
     meta_on.wait()
-    metas[0] = own
     metas_out[...] = metas[...]
     for o in range(NA):
         base = peer(me, NEAR[o], 1) * SLOT
         for r in range(4):
             oh_a[r, o] = slot_rows(base, SLOT, metas_out[r], 1.0, 1.0).astype(BF)
     mix_in.wait()
-    normed(mix_raw, mix_gain, mix, width)
+    normed(raw, mix_gain, mix, width)
+
+    def pick(c, r):
+        picked = jnp.dot(oh_a[r].reshape(NA * SLOT, rows), tok[c, r], preferred_element_type=F32).astype(BF)
+        picked = picked.reshape(NA, SLOT, cw)
+        recv_a[c, 0, r] = picked[0]
+        out_a[c, 1:, r] = picked[1:]
 
     def third(c, _):
-        def pick(r):
-            picked = jnp.dot(oh_a[r].reshape(NA * SLOT, rows), tok[c, r], preferred_element_type=F32).astype(BF)
-            picked = picked.reshape(NA, SLOT, cw)
-            recv_a[c, 0, r] = picked[0]
-            out_a[c, 1:, r] = picked[1:]
-
-        pick(0)
         tok_right(c).wait_recv()
         tok_on_right(c).start()
         tok_left(c).wait_recv()
         tok_on_left(c).start()
+        pick(c, 0)
+        pick(c, 1)
+        pick(c, 2)
+        return 0
+
+    lax.fori_loop(0, NC, third, 0)
+
+    def mix_first(c, _):
         mix_right(c).start()
         mix_left(c).start()
-        pick(1)
-        pick(2)
+        return 0
+
+    lax.fori_loop(0, NC, mix_first, 0)
+
+    def fourth(c, _):
         tok_on_right(c).wait_recv()
         tok_on_left(c).wait_recv()
-        pick(3)
+        pick(c, 3)
         for o in range(1, NA):
             remote(out_a.at[c, o], recv_a.at[c, o], a_s.at[c], a_r.at[c], peer(me, NEAR[o], 1), x).start()
+        return 0
+
+    lax.fori_loop(0, NC, fourth, 0)
+
+    def b_first(c, _):
         b_all(c).wait_recv()
         b_right(c).start()
         b_left(c).start()
         return 0
 
-    lax.fori_loop(0, NC, third, 0)
-
-    def fourth(c, _):
+    lax.fori_loop(0, NC, b_first, 0)
+
+    def mix_second(c, _):
         mix_right(c).wait_recv()
         mix_on_right(c).start()
         mix_left(c).wait_recv()
         mix_on_left(c).start()
+        return 0
+
+    lax.fori_loop(0, NC, mix_second, 0)
+
+    def b_second(c):
         b_right(c).wait_recv()
         b_on_right(c).start()
         b_left(c).wait_recv()
         b_on_left(c).start()
-        return 0
-
-    lax.fori_loop(0, NC, fourth, 0)
+
     for load in loads:
         load.wait()
 
@@ -208,19 +256,45 @@
     def chunk_dots(values, mats, c):
         return [jnp.dot(values, mat[c * cw:(c + 1) * cw], preferred_element_type=F32) for mat in mats]
 
-    for c in range(NC):
+    def steps(c, count, rows_of, sums, store):
+        def step(t, _):
+            g, u = chunk_dots(rows_of(t), (gate_w, up_w), c)
+            if c > 0:
+                g = g + sums[0][t]
+                u = u + sums[1][t]
+            if c < NC - 1:
+                sums[0][t] = g
+                sums[1][t] = u
+            else:
+                store(t, finish(g, u))
+            return 0
+
+        lax.fori_loop(0, count, step, 0)
+
+    def store_a(t, values):
+        hid_a[pl.ds(t * PER, PER)] = values.reshape(PER, 4, SLOT, gate_w.shape[1])
+
+    def store_b(r, values):
+        hid_b[r] = values.reshape(NB, SLOT, gate_w.shape[1])
+
+    def a_steps(c):
         a_all(c).wait_recv()
-
-    def step_a(t, _):
-        total = None
-        for c in range(NC):
-            values = recv_a[c, pl.ds(t * PER, PER)].reshape(PER * 4 * SLOT, cw)
-            parts = chunk_dots(values, (gate_w, up_w), c)
-            total = parts if total is None else [one + two for one, two in zip(total, parts)]
-        hid_a[pl.ds(t * PER, PER)] = finish(*total).reshape(PER, 4, SLOT, gate_w.shape[1])
-        return 0
-
-    lax.fori_loop(0, NA // PER, step_a, 0)
+        steps(
+            c, NA // PER, lambda t: recv_a[c, pl.ds(t * PER, PER)].reshape(PER * 4 * SLOT, cw), (acc_g, acc_u), store_a
+        )
+
+    def b_steps(c):
+        b_on_right(c).wait_recv()
+        b_on_left(c).wait_recv()
+        steps(c, 4, lambda r: recv_b[c, r].reshape(NB * SLOT, cw), (bcc_g, bcc_u), store_b)
+
+    a_steps(0)
+    b_second(0)
+    a_steps(1)
+    b_second(1)
+    b_second(2)
+    a_steps(2)
+    b_second(3)
 
     for c in range(NC):
         mix_on_right(c).wait_recv()
@@ -243,23 +317,11 @@
     halo_next.start()
     halo_prev.start()
 
-    for c in range(NC):
-        b_on_right(c).wait_recv()
-        b_on_left(c).wait_recv()
-
-        def step_b(r, _, c=c):
-            g, u = chunk_dots(recv_b[c, r].reshape(NB * SLOT, cw), (gate_w, up_w), c)
-            if c > 0:
-                g = g + bcc_g[r]
-                u = u + bcc_u[r]
-            if c < NC - 1:
-                bcc_g[r] = g
-                bcc_u[r] = u
-            else:
-                hid_b[r] = finish(g, u).reshape(NB, SLOT, g.shape[1])
-            return 0
-
-        lax.fori_loop(0, 4, step_b, 0)
+    b_steps(0)
+    a_steps(3)
+    b_steps(1)
+    b_steps(2)
+    b_steps(3)
 
     halo_next.wait()
     halo_prev.wait()
@@ -281,9 +343,9 @@
 
 
 def combine_kernel(
-    hid_a, hid_b, metas, down_hbm, mixed, proj_hbm,
+    hid_hbm, hid_b, metas, down_hbm, mixed, proj_hbm,
     out, mix_out,
-    down_w, proj_w, p_a, p_b, bh_in, bf_in, sum_b, ret_a, ret_b, w_a, w_b, p_t, th_in, tf_in, p_m, mh_in, mf_in,
+    hid_a, down_w, proj_w, p_a, p_b, bh_in, bf_in, sum_b, ret_a, ret_b, w_a, w_b, p_t, th_in, tf_in, p_m, mh_in, mf_in,
     bh_s, bh_r, bf_s, bf_r, b_s, b_r, a_s, a_r, th_s, th_r, tf_s, tf_r, mh_s, mh_r, mf_s, mf_r, w_sem,
 ):
     me = lax.axis_index("ep")
@@ -295,9 +357,11 @@
     hb = NB // 2
     down_in = pltpu.make_async_copy(down_hbm, down_w, w_sem.at[0])
     proj_in = pltpu.make_async_copy(proj_hbm, proj_w, w_sem.at[1])
+    hid_in = pltpu.make_async_copy(hid_hbm, hid_a, w_sem.at[2])
+    everyone_in = greet(me, x)
     down_in.start()
+    hid_in.start()
     proj_in.start()
-    greet(me, x)
 
     def cols(c):
         return pl.ds(pl.multiple_of(c * cw, cw), cw)
@@ -342,19 +406,26 @@
     def b_all(c):
         return remote(sum_b.at[c], ret_b.at[c], b_s.at[c], b_r.at[c], me, right)
 
-    down_in.wait()
-
-    def first(c, _):
+    def down_b(c):
         def one(r, _):
             part = jnp.dot(hid_b[r].reshape(NB * SLOT, hid_b.shape[3]), down_w[:, cols(c)], preferred_element_type=F32)
             p_b[c, r] = part.astype(BF).reshape(NB, SLOT, cw)
             return 0
 
         lax.fori_loop(0, 4, one, 0)
+
+    down_in.wait()
+    down_b(0)
+    everyone_in()
+    open_ring(b_ring, 0)
+
+    def first(c, _):
+        down_b(c)
         open_ring(b_ring, c)
         return 0
 
-    lax.fori_loop(0, NC, first, 0)
+    lax.fori_loop(1, NC, first, 0)
+    hid_in.wait()
 
     def second(c, _):
         def one(t, _):
@@ -415,10 +486,15 @@
         open_ring(t_ring, c)
         p_t[c, 0] = weighed(1, c).astype(BF)
         p_t[c, 1] = weighed(2, c).astype(BF)
+        return 0
+
+    lax.fori_loop(0, NC, fourth, 0)
+
+    def fourth_on(c, _):
         pass_on(t_ring, p_t, th_in, c)
         return 0
 
-    lax.fori_loop(0, NC, fourth, 0)
+    lax.fori_loop(0, NC, fourth_on, 0)
 
     def fifth(c, _):
         mix_out[:, cols(c)] = (p_m[c, 0].astype(F32) + arrivals(m_ring, mf_in, c)).astype(BF)
@@ -457,7 +533,7 @@
     return [vmem if place == "v" else anywhere for place in places]
 
 
-def dispatch(moe_in, moe_gain, meta, gate_mat, up_mat, mix_in, mix_gain, proj_b, proj_c, proj_h, taps):
+def dispatch(moe_in, moe_gain, routes, group_logits, pair_logits, gate_mat, up_mat, mix_in, mix_gain, proj_b, proj_c, proj_h, taps):
     rows, width = moe_in.shape
     hidden = gate_mat.shape[1]
     chan = proj_b.shape[1]
@@ -470,17 +546,16 @@
         out_shape=(
             jax.ShapeDtypeStruct((NA, 4, SLOT, hidden), BF),
             jax.ShapeDtypeStruct((4, NB, SLOT, hidden), BF),
-            jax.ShapeDtypeStruct((4,) + meta.shape, F32),
+            jax.ShapeDtypeStruct((4, 8, rows), F32),
             jax.ShapeDtypeStruct((4 * rows, chan), BF),
         ),
-        in_specs=specs("avvaaavaaav"),
+        in_specs=specs("avvvvaaavaaav"),
         out_specs=tuple(specs("vvvv")),
         scratch_shapes=[
             VM((rows, width), BF),
-            VM((rows, width), BF),
             VM((NC, 4, rows, cw), BF),
             VM((NC, 4, rows, cw), BF),
-            VM((4,) + meta.shape, F32),
+            VM((4, 8, rows), F32),
             VM((4, NA, SLOT, rows), BF),
             VM((NB, SLOT, rows), BF),
             VM((NC, NA, 4, SLOT, cw), BF),
@@ -490,6 +565,8 @@
             VM((width, hidden), BF),
             VM((width, hidden), BF),
             VM((3, width, chan), BF),
+            VM((NA // PER, PER * 4 * SLOT, hidden), F32),
+            VM((NA // PER, PER * 4 * SLOT, hidden), F32),
             VM((4, NB * SLOT, hidden), F32),
             VM((4, NB * SLOT, hidden), F32),
             VM((4 * rows + 16, chan), F32),
@@ -499,7 +576,7 @@
         ],
         compiler_params=pltpu.CompilerParams(collective_id=0, **PARAMS),
         cost_estimate=COST,
-    )(moe_in, moe_gain, meta, gate_mat, up_mat, mix_in, mix_gain, proj_b, proj_c, proj_h, taps)
+    )(moe_in, moe_gain, routes, group_logits, pair_logits, gate_mat, up_mat, mix_in, mix_gain, proj_b, proj_c, proj_h, taps)
 
 
 def combine(hid_a, hid_b, metas, down_mat, mixed, proj_out):
@@ -514,9 +591,10 @@
         combine_kernel,
         name="combine",
         out_shape=(jax.ShapeDtypeStruct((rows, width), BF), jax.ShapeDtypeStruct((rows, width), BF)),
-        in_specs=specs("vvvava"),
+        in_specs=specs("avvava"),
         out_specs=tuple(specs("vv")),
         scratch_shapes=[
+            VM((NA, 4, SLOT, hidden), BF),
             VM((hidden, width), BF),
             VM((chan, width), BF),
             VM((NC, NA, 4, SLOT, cw), BF),
@@ -535,7 +613,7 @@
             VM((NC, 2, rows // 2, cw), BF),
             VM((NC, 2, rows, cw), BF),
             pair, pair, pair, pair, single, single, single, single,
-            pair, pair, pair, pair, pair, pair, pair, pair, DMA((2,)),
+            pair, pair, pair, pair, pair, pair, pair, pair, DMA((3,)),
         ],
         compiler_params=pltpu.CompilerParams(collective_id=1, **PARAMS),
         cost_estimate=COST,
@@ -546,24 +624,8 @@
     mix_in, mix_gain, proj_b, proj_c, proj_h, conv_taps, proj_out,
     moe_in, moe_gain, routes, group_logits, pair_logits, expert_gate, expert_up, expert_down,
 ):
-    local_rows, top_count = routes.shape
-    experts_all = lax.axis_size("ep")
-    flat_routes = routes.reshape(-1)
-    route_hits = (flat_routes[:, None] == jnp.arange(experts_all, dtype=jnp.int32)[None, :]).astype(jnp.int32)
-    route_ranks = jnp.sum((jnp.cumsum(route_hits, axis=0) - route_hits) * route_hits, axis=1)
-    slot_ids = (flat_routes * SLOT + route_ranks).reshape(local_rows, top_count)
-    group_prob = jax.nn.softmax(group_logits, axis=-1)
-    member = routes // (experts_all // GROUPS)
-    picked_prob = jnp.sum(
-        group_prob[:, None, :]
-        * (member[:, :, None] == jnp.arange(GROUPS, dtype=jnp.int32)[None, None, :]).astype(F32),
-        axis=-1,
-    )
-    weight = picked_prob * jax.nn.softmax(pair_logits, axis=-1)
-    meta = jnp.concatenate([slot_ids.astype(F32), weight, jnp.zeros((local_rows, 4), F32)], axis=1).T
-
     hid_a, hid_b, metas, mixed = dispatch(
-        moe_in, moe_gain[None, :], meta, expert_gate[0], expert_up[0],
+        moe_in, moe_gain[None, :], routes.T, group_logits.T, pair_logits.T, expert_gate[0], expert_up[0],
         mix_in, mix_gain[None, :], proj_b, proj_c, proj_h, conv_taps,
     )
     moe_out, mix_out = combine(hid_a, hid_b, metas, expert_down[0], mixed, proj_out)

time: 309 us -> 270 us (0.87)
  Pallas kernels: 295 us -> 266 us
  other arithmetic: 6.31 us -> 0 us
    pallas_call x1, Pallas kernels: 154 us -> 137 us  [dispatch(): pl.pallas_call(dispatch_kernel, name='dispatch', out_shape=(jax.ShapeDtyp...]
    pallas_call x1, Pallas kernels: 140 us -> 129 us  [combine(): pl.pallas_call(combine_kernel, name='combine', out_shape=(jax.ShapeDtypeS...]
where the time goes in v3:
time: 270 us
  Pallas kernels  266 us (99%)
  local copies, waits for them, and re-layouts  3.35 us (1%)
    pallas_call x1, Pallas kernels, dispatch(): pl.pallas_call(dispatch_kernel, name='dispatch', out_shape=(jax.ShapeDtyp...  137 us
    pallas_call x1, Pallas kernels, combine(): pl.pallas_call(combine_kernel, name='combine', out_shape=(jax.ShapeDtypeS...  129 us

profile of v3, /device:TPU:1, one launch (start us, length us, event | category | flops | bytes accessed | tf_op | source)
XLA Modules:
  0.0 269.9 jit_solution(14445777548182920603)
XLA Ops:
  0.6 137.4 %dispatch.1 = (bf16[20,4,16,512]{3,2,1,0:T(8,128)(2,1)}, bf16[4,12,16,512]{3,2,1,0:T(8,128)(2,1)}, f32[4,8,128]{2,1,0:T(8,128)}, bf16[512,256]{1,0:T(8,128)(2,1)}) custom-call(bf16[128,4096]{1,0:T(8,128)(2,1)} %moe_hbm.1, f32[1,4096]{1,0:T(1,128)} %bitcast.11, s32[2,128]{1,0:T(2,128)} %bitcast.14, f32[4,128]{1,0:T(4,128)} %bitcast.13, f32[2,128]{1,0:T(2,128)} %bitcast.15, ...), custom_call_target="tpu_custom_call" | custom-call | flops 99999997952 | bytes 12000000 | tf_op jit(solution)/shard_map/dispatch/pallas_call | solution.py:543
  138.0 128.5 %combine.1 = (bf16[128,4096]{1,0:T(8,128)(2,1)}, bf16[128,4096]{1,0:T(8,128)(2,1)}) custom-call(bf16[20,4,16,512]{3,2,1,0:T(8,128)(2,1)} %get-tuple-element.8.hid_hbm, bf16[4,12,16,512]{3,2,1,0:T(8,128)(2,1)} %get-tuple-element.9.hid_b, f32[4,8,128]{2,1,0:T(8,128)} %get-tuple-element.10.metas, bf16[512,4096]{1,0:T(8,128)(2,1)} %bitcast.10, ...), custom_call_target="tpu_custom_call" | custom-call | flops 99999997952 | bytes 12000000 | tf_op jit(solution)/shard_map/combine/pallas_call | solution.py:590
  266.6 0.0 copy-start
  266.6 2.4 copy.19
  268.9 0.0 copy-done
  269.0 1.0 copy.20
Async XLA Ops:
  266.6 2.4 copy-start

commit v4 on v3

--- a/solution.py
+++ b/solution.py
@@ -10,12 +10,15 @@
 F32 = jnp.float32
 MESH = pl.DeviceIdType.MESH
 SLOT = 16
+CAP = 14
+BLOCK = 4 * CAP
+SPACE = 64
 def both(*chips):
     return [(dz, dy, c) for dz, dy in chips for c in (0, 1)]
 
 
-NEAR = both((0, 0), (1, 0), (3, 0), (0, 1), (0, 3)) + [(2, 0, 0), (0, 2, 0)] + both((1, 1), (3, 3), (1, 3), (3, 1))
-FAR = [(2, 0, 1), (0, 2, 1)] + both((2, 1), (2, 3), (1, 2), (3, 2), (2, 2))
+NEAR = both((0, 0), (1, 0), (3, 0), (0, 1), (0, 3), (2, 0), (0, 2), (1, 1), (3, 3), (1, 3), (3, 1))
+FAR = both((2, 1), (2, 3), (1, 2), (3, 2), (2, 2))
 NA = len(NEAR)
 NB = len(FAR)
 NC = 4
@@ -53,6 +56,24 @@
     return jnp.where(meta[0:1] == want, hit0, 0.0) + jnp.where(meta[1:2] == want, hit1, 0.0)
 
 
+def far_rows(me, o, meta, hit0, hit1):
+    return slot_rows(peer(me, FAR[o], 1) * SPACE, SLOT, meta, hit0, hit1).astype(BF)
+
+
+def near_rows(me, o, r, meta, hit0, hit1):
+    return slot_rows(peer(me, NEAR[o], 1) * SPACE - CAP * r, BLOCK, meta, hit0, hit1).astype(BF)
+
+
+def near_steps(do):
+    def one(t, _):
+        do(t * PER, PER)
+        return 0
+
+    lax.fori_loop(0, NA // PER, one, 0)
+    if NA % PER:
+        do(NA - NA % PER, NA % PER)
+
+
 def routing(routes, group_logits, pair_logits):
     count = routes.shape[1]
     r0, r1 = routes[0:1], routes[1:2]
@@ -68,7 +89,7 @@
     group, pair = share(group_logits), share(pair_logits)
 
     def one(route, hit, k):
-        slot = route.astype(F32) * SLOT + jnp.sum(before * hit, axis=0, keepdims=True)
+        slot = route.astype(F32) * SPACE + jnp.sum(before * hit, axis=0, keepdims=True)
         member = sum(
             group[g:g + 1] * jnp.where(jnp.logical_and(route >= 8 * g, route < 8 * g + 8), 1.0, 0.0) for g in range(GROUPS)
         )
@@ -166,7 +187,7 @@
 
     own = metas[0]
     for o in range(NB):
-        oh_b[o] = slot_rows(peer(me, FAR[o], 1) * SLOT, SLOT, own, 1.0, 1.0).astype(BF)
+        oh_b[o] = far_rows(me, o, own, 1.0, 1.0)
 
     def second(c, _):
         picked = jnp.dot(oh_b[...].reshape(NB * SLOT, rows), tok[c, 0], preferred_element_type=F32)
@@ -183,26 +204,25 @@
     meta_on.wait()
     metas_out[...] = metas[...]
     for o in range(NA):
-        base = peer(me, NEAR[o], 1) * SLOT
         for r in range(4):
-            oh_a[r, o] = slot_rows(base, SLOT, metas_out[r], 1.0, 1.0).astype(BF)
+            oh_a[o, :, r * rows:(r + 1) * rows] = near_rows(me, o, r, metas_out[r], 1.0, 1.0)
     mix_in.wait()
     normed(raw, mix_gain, mix, width)
 
-    def pick(c, r):
-        picked = jnp.dot(oh_a[r].reshape(NA * SLOT, rows), tok[c, r], preferred_element_type=F32).astype(BF)
-        picked = picked.reshape(NA, SLOT, cw)
-        recv_a[c, 0, r] = picked[0]
-        out_a[c, 1:, r] = picked[1:]
+    def pick(c):
+        def one(first, count):
+            span = pl.ds(first, count)
+            rows_in = oh_a[span].reshape(count * BLOCK, 4 * rows)
+            picked = jnp.dot(rows_in, tok[c].reshape(4 * rows, cw), preferred_element_type=F32)
+            out_a[c, span] = picked.astype(BF).reshape(count, BLOCK, cw)
+
+        near_steps(one)
 
     def third(c, _):
         tok_right(c).wait_recv()
         tok_on_right(c).start()
         tok_left(c).wait_recv()
         tok_on_left(c).start()
-        pick(c, 0)
-        pick(c, 1)
-        pick(c, 2)
         return 0
 
     lax.fori_loop(0, NC, third, 0)
@@ -217,9 +237,10 @@
     def fourth(c, _):
         tok_on_right(c).wait_recv()
         tok_on_left(c).wait_recv()
-        pick(c, 3)
+        pick(c)
         for o in range(1, NA):
             remote(out_a.at[c, o], recv_a.at[c, o], a_s.at[c], a_r.at[c], peer(me, NEAR[o], 1), x).start()
+        recv_a[c, 0] = out_a[c, 0]
         return 0
 
     lax.fori_loop(0, NC, fourth, 0)
@@ -256,37 +277,35 @@
     def chunk_dots(values, mats, c):
         return [jnp.dot(values, mat[c * cw:(c + 1) * cw], preferred_element_type=F32) for mat in mats]
 
-    def steps(c, count, rows_of, sums, store):
-        def step(t, _):
-            g, u = chunk_dots(rows_of(t), (gate_w, up_w), c)
-            if c > 0:
-                g = g + sums[0][t]
-                u = u + sums[1][t]
-            if c < NC - 1:
-                sums[0][t] = g
-                sums[1][t] = u
-            else:
-                store(t, finish(g, u))
-            return 0
-
-        lax.fori_loop(0, count, step, 0)
-
-    def store_a(t, values):
-        hid_a[pl.ds(t * PER, PER)] = values.reshape(PER, 4, SLOT, gate_w.shape[1])
-
-    def store_b(r, values):
-        hid_b[r] = values.reshape(NB, SLOT, gate_w.shape[1])
+    def step(c, values, sums, at, store):
+        g, u = chunk_dots(values, (gate_w, up_w), c)
+        if c > 0:
+            g = g + sums[0][at]
+            u = u + sums[1][at]
+        if c < NC - 1:
+            sums[0][at] = g
+            sums[1][at] = u
+        else:
+            store[at] = finish(g, u)
 
     def a_steps(c):
         a_all(c).wait_recv()
-        steps(
-            c, NA // PER, lambda t: recv_a[c, pl.ds(t * PER, PER)].reshape(PER * 4 * SLOT, cw), (acc_g, acc_u), store_a
-        )
+
+        def one(first, count):
+            values = recv_a[c, pl.ds(first, count)].reshape(count * BLOCK, cw)
+            step(c, values, (acc_g, acc_u), pl.ds(pl.multiple_of(first * BLOCK, BLOCK), count * BLOCK), hid_a)
+
+        near_steps(one)
 
     def b_steps(c):
         b_on_right(c).wait_recv()
         b_on_left(c).wait_recv()
-        steps(c, 4, lambda r: recv_b[c, r].reshape(NB * SLOT, cw), (bcc_g, bcc_u), store_b)
+
+        def one(r, _):
+            step(c, recv_b[c, r].reshape(NB * SLOT, cw), (bcc_g, bcc_u), r, hid_b)
+            return 0
+
+        lax.fori_loop(0, 4, one, 0)
 
     a_steps(0)
     b_second(0)
@@ -318,11 +337,8 @@
     halo_prev.start()
 
     b_steps(0)
-    a_steps(3)
     b_steps(1)
     b_steps(2)
-    b_steps(3)
-
     halo_next.wait()
     halo_prev.wait()
     cin[0:8] = cin[0:8] * jnp.where(me > 0, 1.0, 0.0)
@@ -331,6 +347,9 @@
     conv = tap[0:1] * cin[7:last + 7] + tap[1:2] * cin[8:last + 8] + tap[2:3] * cin[9:last + 9]
     mixed[...] = (gate_b[...].astype(F32) * conv).astype(BF)
 
+    b_steps(3)
+    a_steps(3)
+
     def drain(c, _):
         for copy in (
             tok_right, tok_left, tok_on_right, tok_on_left, mix_right, mix_left, mix_on_right, mix_on_left,
@@ -345,13 +364,13 @@
 def combine_kernel(
     hid_hbm, hid_b, metas, down_hbm, mixed, proj_hbm,
     out, mix_out,
-    hid_a, down_w, proj_w, p_a, p_b, bh_in, bf_in, sum_b, ret_a, ret_b, w_a, w_b, p_t, th_in, tf_in, p_m, mh_in, mf_in,
+    hid_a, down_w, proj_w, p_a, p_b, bh_in, bf_in, sum_b, ret_a, ret_b, w_a, w_b, p_t, th_in, tf_in, p_m, mh_in, mf_in, acc,
     bh_s, bh_r, bf_s, bf_r, b_s, b_r, a_s, a_r, th_s, th_r, tf_s, tf_r, mh_s, mh_r, mf_s, mf_r, w_sem,
 ):
     me = lax.axis_index("ep")
     x = lax.axis_index("tp")
     right, left = (x + 1) % 4, (x + 3) % 4
-    cw = p_a.shape[4]
+    cw = p_a.shape[3]
     rows = p_t.shape[2]
     half = rows // 2
     hb = NB // 2
@@ -408,7 +427,7 @@
 
     def down_b(c):
         def one(r, _):
-            part = jnp.dot(hid_b[r].reshape(NB * SLOT, hid_b.shape[3]), down_w[:, cols(c)], preferred_element_type=F32)
+            part = jnp.dot(hid_b[r], down_w[:, cols(c)], preferred_element_type=F32)
             p_b[c, r] = part.astype(BF).reshape(NB, SLOT, cw)
             return 0
 
@@ -418,6 +437,20 @@
     down_b(0)
     everyone_in()
     open_ring(b_ring, 0)
+    hid_in.wait()
+
+    def down_a(c):
+        def one(first, count):
+            values = hid_a[pl.ds(pl.multiple_of(first * BLOCK, BLOCK), count * BLOCK)]
+            part = jnp.dot(values, down_w[:, cols(c)], preferred_element_type=F32)
+            p_a[c, pl.ds(first, count)] = part.astype(BF).reshape(count, BLOCK, cw)
+
+        near_steps(one)
+        for o in range(1, NA):
+            remote(p_a.at[c, o], ret_a.at[c, o], a_s.at[c], a_r.at[c], peer(me, NEAR[o], -1), x).start()
+        ret_a[c, 0] = p_a[c, 0]
+
+    down_a(0)
 
     def first(c, _):
         down_b(c)
@@ -425,24 +458,14 @@
         return 0
 
     lax.fori_loop(1, NC, first, 0)
-    hid_in.wait()
+    pass_on(b_ring, p_b, bh_in, 0)
 
     def second(c, _):
-        def one(t, _):
-            span = pl.ds(t * PER, PER)
-            values = hid_a[span].reshape(PER * 4 * SLOT, hid_a.shape[3])
-            part = jnp.dot(values, down_w[:, cols(c)], preferred_element_type=F32)
-            p_a[c, span] = part.astype(BF).reshape(PER, 4, SLOT, cw)
-            return 0
-
-        lax.fori_loop(0, NA // PER, one, 0)
-        for o in range(1, NA):
-            remote(p_a.at[c, o], ret_a.at[c, o], a_s.at[c], a_r.at[c], peer(me, NEAR[o], -1), x).start()
-        ret_a[c, 0] = p_a[c, 0]
+        down_a(c)
         pass_on(b_ring, p_b, bh_in, c)
         return 0
 
-    lax.fori_loop(0, NC, second, 0)
+    lax.fori_loop(1, NC, second, 0)
     proj_in.wait()
 
     def mixer(c, _):
@@ -458,13 +481,12 @@
     lax.fori_loop(0, NC, mixer, 0)
 
     for o in range(NA):
-        base = peer(me, NEAR[o], 1) * SLOT
         for r in range(4):
             meta = metas[r]
-            w_a[r, o] = slot_rows(base, SLOT, meta, meta[2:3], meta[3:4]).astype(BF)
+            w_a[r, o] = near_rows(me, o, r, meta, meta[2:3], meta[3:4])
     for o in range(NB):
         meta = metas[0]
-        w_b[o] = slot_rows(peer(me, FAR[o], 1) * SLOT, SLOT, meta, meta[2:3], meta[3:4]).astype(BF)
+        w_b[o] = far_rows(me, o, meta, meta[2:3], meta[3:4])
 
     def third(c, _):
         sum_b[c] = (p_b[c, 0].astype(F32) + arrivals(b_ring, bf_in, c)).astype(BF)
@@ -477,8 +499,8 @@
     over_rows = (((0,), (0,)), ((), ()))
 
     def weighed(r, c):
-        values = ret_a[c, :, r].reshape(NA * SLOT, cw)
-        return lax.dot_general(w_a[r].reshape(NA * SLOT, rows), values, over_rows, preferred_element_type=F32)
+        values = ret_a[c].reshape(NA * BLOCK, cw)
+        return lax.dot_general(w_a[r].reshape(NA * BLOCK, rows), values, over_rows, preferred_element_type=F32)
 
     def fourth(c, _):
         a_all(c).wait_recv()
@@ -486,6 +508,7 @@
         open_ring(t_ring, c)
         p_t[c, 0] = weighed(1, c).astype(BF)
         p_t[c, 1] = weighed(2, c).astype(BF)
+        acc[c] = weighed(0, c)
         return 0
 
     lax.fori_loop(0, NC, fourth, 0)
@@ -505,7 +528,7 @@
     def sixth(c, _):
         b_all(c).wait_recv()
         values = ret_b[c].reshape(NB * SLOT, cw)
-        total = weighed(0, c) + lax.dot_general(
+        total = acc[c] + lax.dot_general(
             w_b[...].reshape(NB * SLOT, rows), values, over_rows, preferred_element_type=F32
         )
         out[:, cols(c)] = (total + arrivals(t_ring, tf_in, c)).astype(BF)
@@ -544,8 +567,8 @@
         dispatch_kernel,
         name="dispatch",
         out_shape=(
-            jax.ShapeDtypeStruct((NA, 4, SLOT, hidden), BF),
-            jax.ShapeDtypeStruct((4, NB, SLOT, hidden), BF),
+            jax.ShapeDtypeStruct((NA * BLOCK, hidden), BF),
+            jax.ShapeDtypeStruct((4, NB * SLOT, hidden), BF),
             jax.ShapeDtypeStruct((4, 8, rows), F32),
             jax.ShapeDtypeStruct((4 * rows, chan), BF),
         ),
@@ -556,17 +579,17 @@
             VM((NC, 4, rows, cw), BF),
             VM((NC, 4, rows, cw), BF),
             VM((4, 8, rows), F32),
-            VM((4, NA, SLOT, rows), BF),
+            VM((NA, BLOCK, 4 * rows), BF),
             VM((NB, SLOT, rows), BF),
-            VM((NC, NA, 4, SLOT, cw), BF),
+            VM((NC, NA, BLOCK, cw), BF),
             VM((NC, NB, SLOT, cw), BF),
-            VM((NC, NA, 4, SLOT, cw), BF),
+            VM((NC, NA, BLOCK, cw), BF),
             VM((NC, 4, NB, SLOT, cw), BF),
             VM((width, hidden), BF),
             VM((width, hidden), BF),
             VM((3, width, chan), BF),
-            VM((NA // PER, PER * 4 * SLOT, hidden), F32),
-            VM((NA // PER, PER * 4 * SLOT, hidden), F32),
+            VM((NA * BLOCK, hidden), F32),
+            VM((NA * BLOCK, hidden), F32),
             VM((4, NB * SLOT, hidden), F32),
             VM((4, NB * SLOT, hidden), F32),
             VM((4 * rows + 16, chan), F32),
@@ -594,17 +617,17 @@
         in_specs=specs("avvava"),
         out_specs=tuple(specs("vv")),
         scratch_shapes=[
-            VM((NA, 4, SLOT, hidden), BF),
+            VM((NA * BLOCK, hidden), BF),
             VM((hidden, width), BF),
             VM((chan, width), BF),
-            VM((NC, NA, 4, SLOT, cw), BF),
+            VM((NC, NA, BLOCK, cw), BF),
             VM((NC, 4, NB, SLOT, cw), BF),
             VM((NC, 2, hb, SLOT, cw), BF),
             VM((NC, 2, NB, SLOT, cw), BF),
             VM((NC, NB, SLOT, cw), BF),
-            VM((NC, NA, 4, SLOT, cw), BF),
+            VM((NC, NA, BLOCK, cw), BF),
             VM((NC, NB, SLOT, cw), BF),
-            VM((4, NA, SLOT, rows), BF),
+            VM((4, NA, BLOCK, rows), BF),
             VM((NB, SLOT, rows), BF),
             VM((NC, 3, rows, cw), BF),
             VM((NC, 2, rows // 2, cw), BF),
@@ -612,6 +635,7 @@
             VM((NC, 4, rows, cw), BF),
             VM((NC, 2, rows // 2, cw), BF),
             VM((NC, 2, rows, cw), BF),
+            VM((NC, rows, cw), F32),
             pair, pair, pair, pair, single, single, single, single,
             pair, pair, pair, pair, pair, pair, pair, pair, DMA((3,)),
         ],

time: 270 us -> 259 us (0.959)
  Pallas kernels: 266 us -> 255 us
    pallas_call x1, Pallas kernels: 129 us -> 122 us  [combine(): pl.pallas_call(combine_kernel, name='combine', out_shape=(jax.ShapeDtypeS...]
    pallas_call x1, Pallas kernels: 137 us -> 133 us  [dispatch(): pl.pallas_call(dispatch_kernel, name='dispatch', out_shape=(jax.ShapeDtyp...]
where the time goes in v4:
time: 259 us
  Pallas kernels  255 us (98%)
  local copies, waits for them, and re-layouts  3.35 us (1%)
    pallas_call x1, Pallas kernels, dispatch(): pl.pallas_call(dispatch_kernel, name='dispatch', out_shape=(jax.ShapeDtyp...  133 us
    pallas_call x1, Pallas kernels, combine(): pl.pallas_call(combine_kernel, name='combine', out_shape=(jax.ShapeDtypeS...  122 us

profile of v4, /device:TPU:1, one launch (start us, length us, event | category | flops | bytes accessed | tf_op | source)
XLA Modules:
  0.0 258.9 jit_solution(3830942904069049956)
XLA Ops:
  0.6 132.7 %dispatch.1 = (bf16[1232,512]{1,0:T(8,128)(2,1)}, bf16[4,160,512]{2,1,0:T(8,128)(2,1)}, f32[4,8,128]{2,1,0:T(8,128)}, bf16[512,256]{1,0:T(8,128)(2,1)}) custom-call(bf16[128,4096]{1,0:T(8,128)(2,1)} %moe_hbm.1, f32[1,4096]{1,0:T(1,128)} %bitcast.11, s32[2,128]{1,0:T(2,128)} %bitcast.14, f32[4,128]{1,0:T(4,128)} %bitcast.13, f32[2,128]{1,0:T(2,128)} %bitcast.15, ...), custom_call_target="tpu_custom_call" | custom-call | flops 99999997952 | bytes 12000000 | tf_op jit(solution)/shard_map/dispatch/pallas_call | solution.py:566
  133.4 122.1 %combine.1 = (bf16[128,4096]{1,0:T(8,128)(2,1)}, bf16[128,4096]{1,0:T(8,128)(2,1)}) custom-call(bf16[1232,512]{1,0:T(8,128)(2,1)} %get-tuple-element.8.hid_hbm, bf16[4,160,512]{2,1,0:T(8,128)(2,1)} %get-tuple-element.9.hid_b, f32[4,8,128]{2,1,0:T(8,128)} %get-tuple-element.10.metas, bf16[512,4096]{1,0:T(8,128)(2,1)} %bitcast.10, ...), custom_call_target="tpu_custom_call" | custom-call | flops 99999997952 | bytes 12000000 | tf_op jit(solution)/shard_map/combine/pallas_call | solution.py:613
  255.5 0.0 copy-start
  255.5 2.4 copy.19
  257.9 0.0 copy-done
  257.9 1.0 copy.20
Async XLA Ops:
  255.5 2.4 copy-start

commit v5 on v4

--- a/solution.py
+++ b/solution.py
@@ -12,6 +12,7 @@
 SLOT = 16
 CAP = 14
 BLOCK = 4 * CAP
+SPLIT = 14
 SPACE = 64
 def both(*chips):
     return [(dz, dy, c) for dz, dy in chips for c in (0, 1)]
@@ -22,7 +23,7 @@
 NA = len(NEAR)
 NB = len(FAR)
 NC = 4
-PER = 4
+PER = 6
 
 
 def place(x, r):
@@ -149,6 +150,8 @@
     moe_in.wait()
     normed(raw, moe_gain, tok, width)
     mix_in.start()
+    for o in range(NB):
+        oh_b[o] = far_rows(me, o, metas[0], 1.0, 1.0)
     everyone_in()
 
     meta_right = remote(metas.at[0], metas.at[1], meta_s.at[0], meta_r.at[0], me, right)
@@ -171,9 +174,9 @@
     mix_right, mix_left, mix_on_right, mix_on_left = ring(mix, mx_s, mx_r, mxf_s, mxf_r)
     b_right, b_left, b_on_right, b_on_left = ring(recv_b, bx_s, bx_r, bf_s, bf_r)
 
-    def a_all(c):
-        span = pl.ds(1, NA - 1)
-        return remote(out_a.at[c, span], recv_a.at[c, span], a_s.at[c], a_r.at[c], me, right)
+    def a_part(c, part):
+        span = pl.ds(SPLIT, NA - SPLIT) if part else pl.ds(1, SPLIT - 1)
+        return remote(out_a.at[c, span], recv_a.at[c, span], a_s.at[c, part], a_r.at[c, part], me, right)
 
     def b_all(c):
         return remote(out_b.at[c], recv_b.at[c, 0], b_s.at[c], b_r.at[c], me, right)
@@ -183,11 +186,7 @@
         tok_left(c).start()
         return 0
 
-    lax.fori_loop(0, NC, first, 0)
-
-    own = metas[0]
-    for o in range(NB):
-        oh_b[o] = far_rows(me, o, own, 1.0, 1.0)
+    lax.fori_loop(0, NC - 1, first, 0)
 
     def second(c, _):
         picked = jnp.dot(oh_b[...].reshape(NB * SLOT, rows), tok[c, 0], preferred_element_type=F32)
@@ -206,8 +205,6 @@
     for o in range(NA):
         for r in range(4):
             oh_a[o, :, r * rows:(r + 1) * rows] = near_rows(me, o, r, metas_out[r], 1.0, 1.0)
-    mix_in.wait()
-    normed(raw, mix_gain, mix, width)
 
     def pick(c):
         def one(first, count):
@@ -225,7 +222,12 @@
         tok_on_left(c).start()
         return 0
 
-    lax.fori_loop(0, NC, third, 0)
+    third(0, 0)
+    first(NC - 1, 0)
+    lax.fori_loop(1, NC, third, 0)
+
+    mix_in.wait()
+    normed(raw, mix_gain, mix, width)
 
     def mix_first(c, _):
         mix_right(c).start()
@@ -239,7 +241,9 @@
         tok_on_left(c).wait_recv()
         pick(c)
         for o in range(1, NA):
-            remote(out_a.at[c, o], recv_a.at[c, o], a_s.at[c], a_r.at[c], peer(me, NEAR[o], 1), x).start()
+            remote(
+                out_a.at[c, o], recv_a.at[c, o], a_s.at[c, o // SPLIT], a_r.at[c, o // SPLIT], peer(me, NEAR[o], 1), x
+            ).start()
         recv_a[c, 0] = out_a[c, 0]
         return 0
 
@@ -288,14 +292,17 @@
         else:
             store[at] = finish(g, u)
 
-    def a_steps(c):
-        a_all(c).wait_recv()
-
-        def one(first, count):
-            values = recv_a[c, pl.ds(first, count)].reshape(count * BLOCK, cw)
-            step(c, values, (acc_g, acc_u), pl.ds(pl.multiple_of(first * BLOCK, BLOCK), count * BLOCK), hid_a)
-
-        near_steps(one)
+    def a_steps(c, part):
+        a_part(c, part).wait_recv()
+        per = 4 if part else 7
+
+        def one(t, _):
+            first = part * SPLIT + t * per
+            values = recv_a[c, pl.ds(first, per)].reshape(per * BLOCK, cw)
+            step(c, values, (acc_g, acc_u), pl.ds(pl.multiple_of(first * BLOCK, BLOCK), per * BLOCK), hid_a)
+            return 0
+
+        lax.fori_loop(0, 2, one, 0)
 
     def b_steps(c):
         b_on_right(c).wait_recv()
@@ -307,13 +314,16 @@
 
         lax.fori_loop(0, 4, one, 0)
 
-    a_steps(0)
+    a_steps(0, 0)
+    a_steps(0, 1)
     b_second(0)
-    a_steps(1)
     b_second(1)
+    a_steps(1, 0)
+    a_steps(1, 1)
     b_second(2)
-    a_steps(2)
     b_second(3)
+    a_steps(2, 0)
+    a_steps(2, 1)
 
     for c in range(NC):
         mix_on_right(c).wait_recv()
@@ -347,15 +357,18 @@
     conv = tap[0:1] * cin[7:last + 7] + tap[1:2] * cin[8:last + 8] + tap[2:3] * cin[9:last + 9]
     mixed[...] = (gate_b[...].astype(F32) * conv).astype(BF)
 
+    a_steps(3, 0)
     b_steps(3)
-    a_steps(3)
+    a_steps(3, 1)
 
     def drain(c, _):
         for copy in (
             tok_right, tok_left, tok_on_right, tok_on_left, mix_right, mix_left, mix_on_right, mix_on_left,
-            b_all, b_right, b_left, b_on_right, b_on_left, a_all,
+            b_all, b_right, b_left, b_on_right, b_on_left,
         ):
             copy(c).wait_send()
+        a_part(c, 0).wait_send()
+        a_part(c, 1).wait_send()
         return 0
 
     lax.fori_loop(0, NC, drain, 0)
@@ -364,7 +377,7 @@
 def combine_kernel(
     hid_hbm, hid_b, metas, down_hbm, mixed, proj_hbm,
     out, mix_out,
-    hid_a, down_w, proj_w, p_a, p_b, bh_in, bf_in, sum_b, ret_a, ret_b, w_a, w_b, p_t, th_in, tf_in, p_m, mh_in, mf_in, acc,
+    hid_a, down_w, proj_w, p_a, p_b, bh_in, bf_in, sum_b, ret_a, ret_b, w_a, w_b, p_t, th_in, tf_in, p_m, mh_in, mf_in, acc, w_t,
     bh_s, bh_r, bf_s, bf_r, b_s, b_r, a_s, a_r, th_s, th_r, tf_s, tf_r, mh_s, mh_r, mf_s, mf_r, w_sem,
 ):
     me = lax.axis_index("ep")
@@ -484,6 +497,8 @@
         for r in range(4):
             meta = metas[r]
             w_a[r, o] = near_rows(me, o, r, meta, meta[2:3], meta[3:4])
+    for r in range(4):
+        w_t[r] = w_a[r].reshape(NA * BLOCK, rows).T
     for o in range(NB):
         meta = metas[0]
         w_b[o] = far_rows(me, o, meta, meta[2:3], meta[3:4])
@@ -500,7 +515,7 @@
 
     def weighed(r, c):
         values = ret_a[c].reshape(NA * BLOCK, cw)
-        return lax.dot_general(w_a[r].reshape(NA * BLOCK, rows), values, over_rows, preferred_element_type=F32)
+        return jnp.dot(w_t[r], values, preferred_element_type=F32)
 
     def fourth(c, _):
         a_all(c).wait_recv()
@@ -594,7 +609,7 @@
             VM((4, NB * SLOT, hidden), F32),
             VM((4 * rows + 16, chan), F32),
             VM((4 * rows, chan), BF),
-            pair, pair, pair, pair, pair, pair, pair, pair, single, single, pair, pair, pair, pair, single, single,
+            pair, pair, pair, pair, pair, pair, pair, pair, single, single, pair, pair, pair, pair, pair, pair,
             DMA((3,)), DMA((3,)), DMA((2,)), DMA((2,)), DMA((7,)),
         ],
         compiler_params=pltpu.CompilerParams(collective_id=0, **PARAMS),
@@ -636,6 +651,7 @@
             VM((NC, 2, rows // 2, cw), BF),
             VM((NC, 2, rows, cw), BF),
             VM((NC, rows, cw), F32),
+            VM((4, rows, NA * BLOCK), BF),
             pair, pair, pair, pair, single, single, single, single,
             pair, pair, pair, pair, pair, pair, pair, pair, DMA((3,)),
         ],

time: 259 us -> 278 us (1.073)
  the two profiles are of different devices: /device:TPU:1 before, /device:TPU:56 now
where the time goes in v5:
time: 278 us
  Pallas kernels  274 us (99%)
  local copies, waits for them, and re-layouts  3.35 us (1%)
    pallas_call x1, Pallas kernels, combine(): pl.pallas_call(combine_kernel, name='combine', out_shape=(jax.ShapeDtypeS...  145 us
    pallas_call x1, Pallas kernels, dispatch(): pl.pallas_call(dispatch_kernel, name='dispatch', out_shape=(jax.ShapeDtyp...  128 us

profile of v5, /device:TPU:56, one launch (start us, length us, event | category | flops | bytes accessed | tf_op | source)
XLA Modules:
  0.0 277.6 jit_solution(4250768679358473182)
XLA Ops:
  0.6 128.5 %dispatch.1 = (bf16[1232,512]{1,0:T(8,128)(2,1)}, bf16[4,160,512]{2,1,0:T(8,128)(2,1)}, f32[4,8,128]{2,1,0:T(8,128)}, bf16[512,256]{1,0:T(8,128)(2,1)}) custom-call(bf16[128,4096]{1,0:T(8,128)(2,1)} %moe_hbm.1, f32[1,4096]{1,0:T(1,128)} %bitcast.11, s32[2,128]{1,0:T(2,128)} %bitcast.14, f32[4,128]{1,0:T(4,128)} %bitcast.13, f32[2,128]{1,0:T(2,128)} %bitcast.15, ...), custom_call_target="tpu_custom_call" | custom-call | flops 99999997952 | bytes 12000000 | tf_op jit(solution)/shard_map/dispatch/pallas_call | solution.py:581
  129.1 145.1 %combine.1 = (bf16[128,4096]{1,0:T(8,128)(2,1)}, bf16[128,4096]{1,0:T(8,128)(2,1)}) custom-call(bf16[1232,512]{1,0:T(8,128)(2,1)} %get-tuple-element.8.hid_hbm, bf16[4,160,512]{2,1,0:T(8,128)(2,1)} %get-tuple-element.9.hid_b, f32[4,8,128]{2,1,0:T(8,128)} %get-tuple-element.10.metas, bf16[512,4096]{1,0:T(8,128)(2,1)} %bitcast.10, ...), custom_call_target="tpu_custom_call" | custom-call | flops 99999997952 | bytes 12000000 | tf_op jit(solution)/shard_map/combine/pallas_call | solution.py:628
  274.2 0.0 copy-start
  274.2 2.4 copy.19
  276.6 0.0 copy-done
  276.6 1.0 copy.20
Async XLA Ops:
  274.2 2.4 copy-start
